TPU v7x, 32 devices: a whole 2x2x4 slice. The times are simulated.
32 devices in a mesh: ep: 8 (over z, y), tp: 4 (over x, core).
Axes of the slice: x: 2, y: 2, z: 4, core: 2. Of those that a mesh axis runs over, the one named last changes fastest.
Arguments:
- tokens: bfloat16 [1024, 2048], P('ep'), may hold values from -6 to 6
- norm_gain: float32 [2048], replicated, may hold values from 0.1 to 1.9
- routes: int32 [1024, 2], P('ep'), may hold values from 0 to 7, all different within a row; in each aligned block of 128 rows (0 to 127, 128 to 255, ...) at most 48 rows name the same one
- group_prob: float32 [1024], P('ep'), may hold values from 0.2 to 1
- expert_logits: float32 [1024, 2], P('ep'), may hold values from -6 to 6
- gate_weight: bfloat16 [8, 2048, 384], P('ep', None, 'tp'), may hold values from -0.125 to 0.125
- up_weight: bfloat16 [8, 2048, 384], P('ep', None, 'tp'), may hold values from -0.125 to 0.125
- down_matrix: bfloat16 [8, 384, 2048], P('ep', 'tp'), may hold values from -0.3125 to 0.3125
Outputs:
- combined: bfloat16 [1024, 2048], P('ep', 'tp')
Inputs may be any that keep to these rules, and one draw needn't show every extreme that they name: `routes`: each row names 2 different experts. Among the 128 tokens of one index of ep at most 48 rows name one expert, and in every draw some expert is named by exactly 48 of them.
All inputs are finite; a program needn't handle non-finite values.
Results may differ from a plain program's by a relative error of at most 0.013.
Values may be sent and summed in bfloat16 or wider, within the bound.
No kernel may reach another device: no remote copies, remote signals or barrier semaphores. Data moves between devices by JAX's collectives and lax.ppermute only.
A program may use at most 64 MiB of HBM per device.

v0:
```python
import jax
import jax.numpy as jnp
from jax import lax
from jax.sharding import PartitionSpec as P


def hidden_part(buffer, gate_weight, up_weight):
    local_count = gate_weight.shape[0]
    grouped = buffer.reshape(
        buffer.shape[0] // local_count, local_count, buffer.shape[1], buffer.shape[2]
    )
    gate_proj = jnp.einsum(
        "sknd,kdf->sknf", grouped, gate_weight, preferred_element_type=jnp.float32
    )
    up_proj = jnp.einsum("sknd,kdf->sknf", grouped, up_weight, preferred_element_type=jnp.float32)
    hidden_state = (jax.nn.silu(gate_proj) * up_proj).astype(jnp.bfloat16)
    return hidden_state.reshape(buffer.shape[0], buffer.shape[1], hidden_state.shape[3])


def down_blocks(hidden_full, down_cols, block_count):
    local_count = down_cols.shape[0]
    width = hidden_full.shape[2] // block_count
    grouped = hidden_full.reshape(
        hidden_full.shape[0] // local_count, local_count, hidden_full.shape[1], block_count, width
    )
    columns = down_cols.reshape(local_count, block_count, width, down_cols.shape[2])
    block_list = jnp.einsum(
        "sknrf,krfd->sknrd", grouped, columns, preferred_element_type=jnp.float32
    ).astype(jnp.bfloat16)
    summed = jnp.sum(block_list.astype(jnp.float32), 3).astype(jnp.bfloat16)
    return summed.reshape(hidden_full.shape[0], hidden_full.shape[1], down_cols.shape[2])


def body(tokens, norm_gain, routes, group_prob, expert_logits, gate_weight, up_weight, down_matrix):
    tok_rows, model_width = tokens.shape
    top_count = routes.shape[1]
    experts = gate_weight.shape[0] * lax.axis_size("ep")
    capacity = 3 * top_count * tok_rows // (2 * experts)
    block_count = lax.axis_size("tp")
    down_cols = lax.all_to_all(down_matrix, "tp", split_axis=2, concat_axis=1, tiled=True)
    values = tokens.astype(jnp.float32)
    normed = (
        values * lax.rsqrt(jnp.mean(values * values, -1, keepdims=True) + 1e-06) * norm_gain
    ).astype(jnp.bfloat16)
    flat_ids = routes.reshape(-1)
    onehot = (flat_ids[:, None] == jnp.arange(experts, dtype=jnp.int32)[None, :]).astype(jnp.int32)
    earlier = jnp.cumsum(onehot, 0) - onehot
    slot_index = jnp.sum(earlier * onehot, 1)
    target = flat_ids * capacity + slot_index
    owners = jnp.arange(tok_rows * top_count, dtype=jnp.int32) // top_count
    outgoing = (
        jnp.zeros((experts * capacity, model_width), jnp.bfloat16).at[target].set(normed[owners])
    )
    outgoing = outgoing.reshape(experts, capacity, model_width)
    hidden_state = hidden_part(
        lax.all_to_all(outgoing, "ep", split_axis=0, concat_axis=0, tiled=True),
        gate_weight,
        up_weight,
    )
    hidden_full = lax.all_gather(hidden_state, "tp", axis=2, tiled=True)
    summed = down_blocks(hidden_full, down_cols, block_count)
    returned = lax.all_to_all(summed, "ep", split_axis=0, concat_axis=0, tiled=True)
    flat_back = returned.reshape(experts * capacity, returned.shape[2])
    weights = group_prob[:, None] * jax.nn.softmax(expert_logits, axis=-1)
    picked = flat_back[target].reshape(tok_rows, top_count, flat_back.shape[1]).astype(jnp.float32)
    combined = jnp.sum(picked * weights[:, :, None], 1).astype(jnp.bfloat16)
    return combined


def solution(mesh):
    return jax.shard_map(
        body,
        mesh=mesh,
        in_specs=(
            P("ep", None),
            P(),
            P("ep", None),
            P("ep"),
            P("ep", None),
            P("ep", None, "tp"),
            P("ep", None, "tp"),
            P("ep", "tp", None),
        ),
        out_specs=P("ep", "tp"),
        check_vma=False,
    )
```

profile of v0, /device:TPU:0, one launch (start us, length us, event | category | flops | bytes accessed | tf_op | source)
XLA Modules:
  0.0 104.3 jit_solution(11414660805682031129)
XLA Ops:
  0.0 2.4 %copy.32 = bf16[1,96,2048]{1,0,2:T(2,128)(2,1)S(1)} copy(bf16[1,96,2048]{2,1,0:T(8,128)(2,1)} %param.15) | data formatting | bytes 786432 | tf_op args[7]
  2.4 0.5 broadcast.137
  2.9 11.6 %reduce.6 = bf16[2048,96]{1,0:T(8,128)(2,1)S(1)} reduce(bf16[2048,1,96]{2,1,0:T(2,128)(2,1)S(1)} %bitcast.53, bf16[]{:T(256)} %broadcast.137), dimensions={1}, to_apply=%bitcast.44.reduce_sub_computation | reduce | bytes 786434
  14.5 1.6 %reshape.188 = bf16[4,2,24576]{2,1,0:T(2,128)(2,1)} reshape(bf16[2048,96]{1,0:T(8,128)(2,1)S(1)} %reduce.6) | data formatting | bytes 786432
  16.1 4.2 %all-to-all-start = ((bf16[4,2,24576]{2,1,0:T(2,128)(2,1)}), bf16[4,2,24576]{2,1,0:T(2,128)(2,1)S(1)}, u32[]{:S(2)}, u32[]{:S(2)}) async-start(bf16[4,2,24576]{2,1,0:T(2,128)(2,1)} %reshape.188), calls=%async_computation | async-start | bytes 786432 | tf_op jit(solution)/shard_map/all_to_all | solution.py:40
  20.7 0.6 reduce-window.6
  22.4 6.7 %scatter_custom_fusion = bf16[384,2048]{1,0:T(8,128)(2,1)} fusion(s32[256]{0:T(256)S(1)} %bitcast.57, bf16[128,2048]{1,0:T(8,128)(2,1)S(1)} %fusion.4, s32[1024]{0:T(1024)S(1)} %pad_clamp_fusion.1, bf16[]{:T(256)} %constant.32.clone.1), kind=kCustom, calls=%fused_computation.13 | custom fusion | bytes 1572866 | tf_op jit(solution)/shard_map/scatter | solution.py:52
  29.1 6.7 %all-to-all-start.1 = ((bf16[8,48,2048]{2,1,0:T(8,128)(2,1)}), bf16[8,48,2048]{2,1,0:T(8,128)(2,1)S(1)}, u32[]{:S(2)}, u32[]{:S(2)}) async-start(bf16[8,48,2048]{2,1,0:T(8,128)(2,1)} %bitcast.6), calls=%async_computation.1 | async-start | bytes 3145728 | tf_op jit(solution)/shard_map/all_to_all | solution.py:56
  35.9 0.8 reshape.189
  36.6 1.9 %fusion.14 = (bf16[1,96,512]{1,0,2:T(2,128)(2,1)}, bf16[1,96,512]{1,0,2:T(2,128)(2,1)S(1)}, bf16[1,96,512]{1,0,2:T(2,128)(2,1)S(1)}, bf16[1,96,512]{1,0,2:T(2,128)(2,1)}) fusion(bf16[1,96,2048]{1,0,2:T(2,128)(2,1)S(1)} %bitcast.52), kind=kLoop, calls=%fused_computation.40 | loop fusion | bytes 786432 | tf_op jit(solution)/shard_map/slice.2
  38.5 1.1 %copy.33 = bf16[1,96,512]{2,1,0:T(8,128)(2,1)S(1)} copy(bf16[1,96,512]{1,0,2:T(2,128)(2,1)} %get-tuple-element.5) | data formatting | bytes 196608 | tf_op jit(solution)/shard_map/slice.2
  39.6 1.1 %copy.34 = bf16[1,96,512]{2,1,0:T(8,128)(2,1)S(1)} copy(bf16[1,96,512]{1,0,2:T(2,128)(2,1)} %get-tuple-element.8) | data formatting | bytes 196608 | tf_op jit(solution)/shard_map/slice.3
  41.0 32.3 %all-to-all-done.1 = bf16[8,48,2048]{2,1,0:T(8,128)(2,1)S(1)} async-done(((bf16[8,48,2048]{2,1,0:T(8,128)(2,1)}), bf16[8,48,2048]{2,1,0:T(8,128)(2,1)S(1)}, u32[]{:S(2)}, u32[]{:S(2)}) %all-to-all-start.1) | async-done | bytes 1572896 | tf_op jit(solution)/shard_map/all_to_all | solution.py:56
  73.3 0.6 convolution_bitcast_fusion.1
  73.9 0.6 fusion.1
  74.6 8.7 %all-gather = bf16[8,1,48,384]{2,0,1,3:T(8,128)(2,1)S(1)} all-gather(bf16[8,1,48,96]{2,0,1,3:T(8,128)(2,1)S(1)} %copy.40), channel_id=2, replica_groups=mesh['ep'=8,'tp'=4] {'tp'}, dimensions={3}, use_global_device_ids=true | all-gather | bytes 368640 | tf_op jit(solution)/shard_map/all_gather | solution.py:60
  83.4 0.5 copy.42
  83.9 0.5 fusion.15
  84.4 1.1 %convert_reduce_fusion = bf16[512,8,48]{0,2,1:T(8,128)(2,1)} fusion(f32[4,512,8,48]{1,3,2,0:T(8,128)S(1)} %bitcast.51), kind=kLoop, calls=%fused_computation.3 | loop fusion | flops 1376256 | bytes 3538944 | tf_op jit(solution)/shard_map/reduce_sum | solution.py:30
  85.6 3.6 %all-to-all-start.2 = ((bf16[8,48,512]{2,1,0:T(8,128)(2,1)}), bf16[8,48,512]{2,1,0:T(8,128)(2,1)S(1)}, u32[]{:S(2)}, u32[]{:S(2)}) async-start(bf16[8,48,512]{2,1,0:T(8,128)(2,1)} %bitcast.23), calls=%async_computation.2 | async-start | bytes 786432 | tf_op jit(solution)/shard_map/all_to_all | solution.py:62
  89.4 12.0 %all-to-all-done.2 = bf16[8,48,512]{2,1,0:T(8,128)(2,1)S(1)} async-done(((bf16[8,48,512]{2,1,0:T(8,128)(2,1)}), bf16[8,48,512]{2,1,0:T(8,128)(2,1)S(1)}, u32[]{:S(2)}, u32[]{:S(2)}) %all-to-all-start.2) | async-done | bytes 393248 | tf_op jit(solution)/shard_map/all_to_all | solution.py:62
  101.4 1.2 %gather_fusion = bf16[256,512]{1,0:T(8,128)(2,1)S(1)} fusion(bf16[384,512]{1,0:T(8,128)(2,1)S(1)} %bitcast.50, s32[1024]{0:T(1024)S(1)} %pad_clamp_fusion), kind=kCustom, calls=%fused_computation.1 | custom fusion | bytes 525312 | tf_op jit(solution)/shard_map/gather | solution.py:65
  102.6 0.3 reshape.150
  102.9 1.4 %multiply_reduce_fusion = bf16[128,512]{1,0:T(8,128)(2,1)} fusion(f32[128,2,512]{2,1,0:T(2,128)S(1)} %reshape.150, f32[128,2]{1,0:T(8,128)S(1)} %copy.43), kind=kLoop, calls=%fused_computation.16 | loop fusion | flops 196608 | bytes 656384 | tf_op jit(solution)/shard_map/reduce_sum | solution.py:66
  (41 shorter events, 2.1 us)
Async XLA Ops:
  0.0 73.3 %copy-start = (bf16[1,2048,96]{1,2,0:T(8,128)(2,1)S(1)}, bf16[1,2048,96]{1,2,0:T(8,128)(2,1)}, u32[]{:S(2)}) copy-start(bf16[1,2048,96]{1,2,0:T(8,128)(2,1)} %param.13) | copy-start | bytes 1179652
  2.9 17.4 %copy-start.4 = (s32[128,2]{0,1:T(2,128)S(1)}, s32[128,2]{0,1:T(2,128)}, u32[]{:S(2)}) copy-start(s32[128,2]{0,1:T(2,128)} %param.10) | copy-start | bytes 3076
  2.9 19.0 %copy-start.1 = (bf16[128,2048]{1,0:T(8,128)(2,1)S(1)}, bf16[128,2048]{1,0:T(8,128)(2,1)}, u32[]{:S(2)}) copy-start(bf16[128,2048]{1,0:T(8,128)(2,1)} %param.8) | copy-start | bytes 1572868
  14.5 7.6 %copy-start.3 = (f32[2048]{0:T(1024)S(1)}, f32[2048]{0:T(1024)}, u32[]{:S(2)}) copy-start(f32[2048]{0:T(1024)} %param.9) | copy-start | bytes 24580
  16.1 13.1 %all-to-all-start = ((bf16[4,2,24576]{2,1,0:T(2,128)(2,1)}), bf16[4,2,24576]{2,1,0:T(2,128)(2,1)S(1)}, u32[]{:S(2)}, u32[]{:S(2)}) async-start(bf16[4,2,24576]{2,1,0:T(2,128)(2,1)} %reshape.188), calls=%async_computation | async-start | bytes 786432 | tf_op jit(solution)/shard_map/all_to_all | solution.py:40
  29.1 44.2 %all-to-all-start.1 = ((bf16[8,48,2048]{2,1,0:T(8,128)(2,1)}), bf16[8,48,2048]{2,1,0:T(8,128)(2,1)S(1)}, u32[]{:S(2)}, u32[]{:S(2)}) async-start(bf16[8,48,2048]{2,1,0:T(8,128)(2,1)} %bitcast.6), calls=%async_computation.1 | async-start | bytes 3145728 | tf_op jit(solution)/shard_map/all_to_all | solution.py:56
  40.9 33.0 %copy-start.6 = (bf16[1,2048,96]{1,2,0:T(8,128)(2,1)S(1)}, bf16[1,2048,96]{1,2,0:T(8,128)(2,1)}, u32[]{:S(2)}) copy-start(bf16[1,2048,96]{1,2,0:T(8,128)(2,1)} %param.14) | copy-start | bytes 1179652
  84.4 4.8 %copy-start.2 = (f32[128,2]{0,1:T(2,128)S(1)}, f32[128,2]{0,1:T(2,128)}, u32[]{:S(2)}) copy-start(f32[128,2]{0,1:T(2,128)} %param.12) | copy-start | bytes 3076
  84.4 4.8 %copy-start.5 = (f32[128]{0:T(128)S(1)}, f32[128]{0:T(128)}, u32[]{:S(2)}) copy-start(f32[128]{0:T(128)} %param.11) | copy-start | bytes 1540
  85.6 15.9 %all-to-all-start.2 = ((bf16[8,48,512]{2,1,0:T(8,128)(2,1)}), bf16[8,48,512]{2,1,0:T(8,128)(2,1)S(1)}, u32[]{:S(2)}, u32[]{:S(2)}) async-start(bf16[8,48,512]{2,1,0:T(8,128)(2,1)} %bitcast.23), calls=%async_computation.2 | async-start | bytes 786432 | tf_op jit(solution)/shard_map/all_to_all | solution.py:62
where the time goes:
time: 105 us; the launch traced here: 104 us
  waiting for transfers between devices  44.4 us (42%)
  local copies, waits for them, and re-layouts  19.4 us (18%)
  other arithmetic  15.3 us (15%)
  starting transfers between devices  14.6 us (14%)
  blocking collectives  8.74 us (8%)
  matrix products  1.68 us (2%)
    all_to_all x1, waiting for transfers between devices, body(): lax.all_to_all(outgoing, 'ep', split_axis=0, concat_axis=0, tiled=True)  32.3 us
    all_to_all x1, waiting for transfers between devices, body(): lax.all_to_all(summed, 'ep', split_axis=0, concat_axis=0, tiled=True)  12 us
    unnamed x1, other arithmetic  11.6 us
    all_gather x1, blocking collectives, body(): hidden_full = lax.all_gather(hidden_state, 'tp', axis=2, tiled=True)  8.74 us
    scatter x1, local copies, waits for them, and re-layouts, body(): jnp.zeros((experts * capacity, model_width), jnp.bfloat16).at[target]  6.74 us
    all_to_all x1, starting transfers between devices, body(): lax.all_to_all(outgoing, 'ep', split_axis=0, concat_axis=0, tiled=True)  6.73 us
    unnamed x19, local copies, waits for them, and re-layouts  5.36 us
    another operation x7, local copies, waits for them, and re-layouts  4.77 us
  transfers between devices with their start and end apart: 3, of which 2 were waited for; matrix products, arithmetic and copies ran while one was open for 13% of the time, Pallas kernels for 0%

commit v1 on v0

v1 whole, which is shorter than its diff:
```python
import functools

import jax
import jax.numpy as jnp
from jax import lax
from jax.experimental import pallas as pl
from jax.experimental.pallas import tpu as pltpu
from jax.sharding import PartitionSpec as P

F32, BF16, I32 = jnp.float32, jnp.bfloat16, jnp.int32
VM = pl.BlockSpec(memory_space=pltpu.VMEM)
SM = pl.BlockSpec(memory_space=pltpu.SMEM)


def dot(a, b, ca, cb):
    return lax.dot_general(a, b, (((ca,), (cb,)), ((), ())), preferred_element_type=F32)


def slot_tables(routes, experts, capacity):
    top, count = routes.shape
    expert_of = lax.broadcasted_iota(I32, (experts, count), 0)
    named = routes[0:1] == expert_of
    for k in range(1, top):
        named = named | (routes[k : k + 1] == expert_of)
    ahead = lax.broadcasted_iota(I32, (count, count), 0) < lax.broadcasted_iota(
        I32, (count, count), 1
    )
    ones = jnp.where(named, 1.0, 0.0).astype(BF16)
    earlier = dot(ones, jnp.where(ahead, 1.0, 0.0).astype(BF16), 1, 0)
    place = jnp.where(named, earlier, -1.0).astype(BF16)
    slots = experts * capacity
    inside = lax.broadcasted_iota(I32, (slots, experts), 0) - capacity * lax.broadcasted_iota(
        I32, (slots, experts), 1
    )
    owned = (inside >= 0) & (inside < capacity)
    spread = jnp.where(owned, 1.0, 0.0).astype(BF16)
    own_place = jnp.sum(jnp.where(owned, inside, 0), 1, keepdims=True).astype(F32)
    held = dot(spread, place, 1, 0) == own_place
    return spread, held


def dispatch_kernel(experts, capacity, at_ref, tokens_ref, gain_ref, routes_ref, out_ref):
    width = out_ref.shape[1]
    values = tokens_ref[...].astype(F32)
    scale = lax.rsqrt(jnp.mean(values * values, -1, keepdims=True) + 1e-06)
    here = pl.ds(pl.multiple_of(at_ref[0] * width, width), width)
    normed = (tokens_ref[:, here].astype(F32) * scale * gain_ref[:, here]).astype(BF16)
    _, held = slot_tables(routes_ref[...], experts, capacity)
    picks = jnp.where(held, 1.0, 0.0).astype(BF16)
    out_ref[...] = dot(picks, normed, 1, 0).astype(BF16)


def gates_kernel(experts, capacity, routes_ref, prob_ref, logits_ref, out_ref):
    routes, logits = routes_ref[...], logits_ref[...]
    top, count = routes.shape
    powers = jnp.exp(logits - jnp.max(logits, 0, keepdims=True))
    weights = prob_ref[...] * (powers / jnp.sum(powers, 0, keepdims=True))
    spread, held = slot_tables(routes, experts, capacity)
    expert_of = lax.broadcasted_iota(I32, (experts, count), 0)
    by_expert = jnp.zeros((experts, count), F32)
    for k in range(top):
        by_expert = by_expert + jnp.where(routes[k : k + 1] == expert_of, weights[k : k + 1], 0.0)
    high = by_expert.astype(BF16)
    low = (by_expert - high.astype(F32)).astype(BF16)
    slots = held.shape[0]
    out_ref[0:slots] = jnp.where(held, dot(spread, high, 1, 0), 0.0).astype(BF16)
    out_ref[slots:] = jnp.where(held, dot(spread, low, 1, 0), 0.0).astype(BF16)


def project_kernel(at_ref, mine_ref, other_ref, gate_ref, up_ref, got_ref, full_ref, send_ref):
    width = mine_ref.shape[1]
    here = pl.ds(pl.multiple_of(at_ref[0] * width, width), width)
    there = pl.ds(pl.multiple_of(at_ref[1] * width, width), width)
    near = pl.ds(pl.multiple_of(at_ref[2] * width, width), width)
    far = pl.ds(pl.multiple_of(at_ref[3] * width, width), width)
    first = jnp.concatenate(
        [gate_ref[:, here], up_ref[:, here], got_ref[0, :, near], got_ref[1, :, near]], 0
    )
    second = jnp.concatenate(
        [gate_ref[:, there], up_ref[:, there], got_ref[0, :, far], got_ref[1, :, far]], 0
    )
    total = dot(first, mine_ref[...], 1, 1) + dot(second, other_ref[...], 1, 1)
    full_ref[...] = total
    send_ref[...] = total.astype(BF16)


def hidden_kernel(full_ref, got_ref, out_ref):
    rows = out_ref.shape[0] // 2
    for half in range(2):
        a, b = 2 * rows * half, 2 * rows * (1 - half)
        gate = full_ref[a : a + rows] + got_ref[b : b + rows].astype(F32)
        up = full_ref[a + rows : a + 2 * rows] + got_ref[b + rows : b + 2 * rows].astype(F32)
        out_ref[rows * half : rows * (half + 1)] = (gate / (1.0 + jnp.exp(-gate)) * up).astype(BF16)


def down_kernel(at_ref, mine_ref, other_ref, down_ref, got_ref, pair_ref, out_ref):
    width = out_ref.shape[1]
    here = pl.ds(pl.multiple_of(at_ref[0] * width, width), width)
    near = pl.ds(pl.multiple_of(at_ref[2] * width, width), width)
    hidden = jnp.concatenate([mine_ref[...], other_ref[...]], 0)
    columns = jnp.concatenate([down_ref[:, here], got_ref[2, :, near], pair_ref[...]], 0)
    out_ref[...] = dot(hidden, columns, 0, 0).astype(BF16)


def combine_kernel(gates_ref, back_ref, out_ref):
    slots = back_ref.shape[0]
    back = back_ref[...]
    total = dot(gates_ref[0:slots], back, 0, 0) + dot(gates_ref[slots:], back, 0, 0)
    out_ref[...] = total.astype(BF16)


def call(kernel, shapes, scalars, arrays, name):
    return pl.pallas_call(
        kernel,
        out_shape=shapes,
        in_specs=[SM] * len(scalars) + [VM] * len(arrays),
        out_specs=jax.tree.map(lambda _: VM, shapes),
        name=name,
    )(*scalars, *arrays)


def body(tokens, norm_gain, routes, group_prob, expert_logits, gate_weight, up_weight, down_matrix):
    tok_rows, model_width = tokens.shape
    top = routes.shape[1]
    local, _, block = gate_weight.shape
    ep, tp = lax.axis_size("ep"), lax.axis_size("tp")
    experts = local * ep
    capacity = 3 * top * tok_rows // (2 * experts)
    slots = experts * capacity
    width = model_width // tp
    shape = jax.ShapeDtypeStruct

    q = lax.axis_index("tp").astype(I32)
    at = jnp.stack([q, q ^ 1, q % 2, 1 - q % 2])
    near = [(i, i ^ 1) for i in range(tp)]
    far = [(i, i ^ 2) for i in range(tp)]

    gate, up, down = gate_weight[0].T, up_weight[0].T, down_matrix[0]
    away = (1 - q // 2) * (2 * width)
    packed = jnp.stack(
        [lax.dynamic_slice_in_dim(w, away, 2 * width, 1) for w in (gate, up, down)]
    )
    got = lax.ppermute(packed, "tp", far)

    outgoing = call(
        functools.partial(dispatch_kernel, experts, capacity),
        shape((slots, width), BF16),
        [at],
        [tokens, norm_gain[None], routes.T],
        "dispatch",
    )
    mine = lax.all_to_all(
        outgoing.reshape(ep, slots // ep, width), "ep", split_axis=0, concat_axis=0, tiled=True
    ).reshape(slots, width)
    gates = call(
        functools.partial(gates_kernel, experts, capacity),
        shape((2 * slots, tok_rows), BF16),
        [],
        [routes.T, group_prob[None], expert_logits.T],
        "gates",
    )
    pair = lax.ppermute(
        jnp.concatenate(
            [
                lax.dynamic_slice_in_dim(down, at[1] * width, width, 1),
                lax.dynamic_slice_in_dim(got[2], at[3] * width, width, 1),
            ],
            0,
        ),
        "tp",
        near,
    )
    other = lax.ppermute(mine, "tp", near)
    full, send = call(
        project_kernel,
        (shape((4 * block, slots), F32), shape((4 * block, slots), BF16)),
        [at],
        [mine, other, gate, up, got],
        "project",
    )
    hidden = call(
        hidden_kernel,
        shape((2 * block, slots), BF16),
        [],
        [full, lax.ppermute(send, "tp", far)],
        "hidden",
    )
    summed = call(
        down_kernel,
        shape((slots, width), BF16),
        [at],
        [hidden, lax.ppermute(hidden, "tp", near), down, got, pair],
        "down",
    )
    back = lax.all_to_all(
        summed.reshape(ep, slots // ep, width), "ep", split_axis=0, concat_axis=0, tiled=True
    ).reshape(slots, width)
    return call(combine_kernel, shape((tok_rows, width), BF16), [], [gates, back], "combine")


def solution(mesh):
    return jax.shard_map(
        body,
        mesh=mesh,
        in_specs=(
            P("ep", None),
            P(),
            P("ep", None),
            P("ep"),
            P("ep", None),
            P("ep", None, "tp"),
            P("ep", None, "tp"),
            P("ep", "tp", None),
        ),
        out_specs=P("ep", "tp"),
        check_vma=False,
    )
```

time: 105 us -> 66.4 us (0.63)
  other arithmetic: 15.3 us -> 0.74 us
  local copies, waits for them, and re-layouts: 19.4 us -> 4.97 us
  waiting for transfers between devices: 44.4 us -> 30.4 us
  Pallas kernels: 0 us -> 13.6 us
  blocking collectives: 8.74 us -> 0 us
  matrix products: 1.68 us -> 0 us
  starting transfers between devices: 14.6 us -> 16 us
    all_to_all x3 -> x2, waiting for transfers between devices: 44.4 us -> 19.3 us  [the longest x1 10.3 us: body(): lax.all_to_all(summed.reshape(ep, slots // ep, width), 'ep', split_axis=0...]
    pallas_call x0 -> x6, Pallas kernels: none -> 13.6 us  [call(): pl.pallas_call(kernel, out_shape=shapes, in_specs=[SM] * len(scalars) + [...]
    unnamed x1 -> x0, other arithmetic: 11.6 us -> none
    ppermute x0 -> x5, waiting for transfers between devices: none -> 11.1 us  [the longest x1 5.28 us: body(): lax.ppermute(send, 'tp', far)]
    all_gather x1 -> x0, blocking collectives: 8.74 us -> none  [body(): hidden_full = lax.all_gather(hidden_state, 'tp', axis=2, tiled=True)]
    scatter x1 -> x0, local copies, waits for them, and re-layouts: 6.74 us -> none  [body(): jnp.zeros((experts * capacity, model_width), jnp.bfloat16).at[target]]
    another operation x7 -> x1, local copies, waits for them, and re-layouts: 4.77 us -> 0.03 us  [body(): jnp.stack([lax.dynamic_slice_in_dim(w, away, 2 * width, 1) for w in (gate...]
    ppermute x0 -> x5, starting transfers between devices: none -> 3.13 us  [the longest x1 1.56 us: body(): got = lax.ppermute(packed, 'tp', far)]
  transfers between devices with their start and end apart: 3 -> 7, of which waited for: 2 -> 5; matrix products, arithmetic and copies ran while one was open for 13% -> 0% of each run, Pallas kernels for 0% -> 6%
where the time goes in v1:
time: 66.4 us; the launch traced here: 65.9 us
  waiting for transfers between devices  30.4 us (46%)
  starting transfers between devices  16 us (24%)
  Pallas kernels  13.6 us (20%)
  local copies, waits for them, and re-layouts  4.97 us (7%)
  other arithmetic  0.74 us (1%)
    pallas_call x6, Pallas kernels, call(): pl.pallas_call(kernel, out_shape=shapes, in_specs=[SM] * len(scalars) + [...  13.6 us
    all_to_all x1, waiting for transfers between devices, body(): lax.all_to_all(summed.reshape(ep, slots // ep, width), 'ep', split_axis=0...  10.3 us
    all_to_all x1, waiting for transfers between devices, body(): lax.all_to_all(outgoing.reshape(ep, slots // ep, width), 'ep', split_axis...  9.02 us
    all_to_all x1, starting transfers between devices, body(): lax.all_to_all(outgoing.reshape(ep, slots // ep, width), 'ep', split_axis...  7.44 us
    all_to_all x1, starting transfers between devices, body(): lax.all_to_all(summed.reshape(ep, slots // ep, width), 'ep', split_axis=0...  5.44 us
    ppermute x1, waiting for transfers between devices, body(): lax.ppermute(send, 'tp', far)  5.28 us
    ppermute x1, waiting for transfers between devices, body(): got = lax.ppermute(packed, 'tp', far)  4.28 us
    unnamed x20, local copies, waits for them, and re-layouts  3.99 us
  transfers between devices with their start and end apart: 7, of which 5 were waited for; matrix products, arithmetic and copies ran while one was open for 0% of the time, Pallas kernels for 6%

profile of v1, /device:TPU:0, one launch (start us, length us, event | category | flops | bytes accessed | tf_op | source)
XLA Modules:
  0.0 65.9 jit_solution(17822093830256259416)
XLA Ops:
  0.0 0.7 pad_add_fusion.at_ref
  0.7 2.3 %dispatch.1 = bf16[384,512]{1,0:T(8,128)(2,1)} custom-call(s32[4]{0:T(128)} %pad_add_fusion.at_ref, bf16[128,2048]{1,0:T(8,128)(2,1)} %tokens_ref.1, f32[1,2048]{1,0:T(1,128)} %bitcast.43, s32[2,128]{1,0:T(2,128)} %bitcast.44), custom_call_target="tpu_custom_call" | custom-call | tf_op jit(solution)/shard_map/dispatch/pallas_call | solution.py:113
  3.0 7.4 %all-to-all-start = ((bf16[8,48,512]{2,1,0:T(8,128)(2,1)}), bf16[8,48,512]{2,1,0:T(8,128)(2,1)S(1)}, u32[]{:S(2)}, u32[]{:S(2)}) async-start(bf16[8,48,512]{2,1,0:T(8,128)(2,1)} %bitcast.37), calls=%async_computation | async-start | bytes 786432 | tf_op jit(solution)/shard_map/all_to_all | solution.py:152
  10.5 0.9 %copy-done.4 = bf16[1,2048,96]{1,2,0:T(8,128)(2,1)S(1)} copy-done((bf16[1,2048,96]{1,2,0:T(8,128)(2,1)S(1)}, bf16[1,2048,96]{1,2,0:T(8,128)(2,1)}, u32[]{:S(2)}) %copy-start.4) | copy-done | bytes 393240
  11.5 1.6 %collective-permute-start.1 = (bf16[3,96,1024]{2,1,0:T(8,128)(2,1)S(1)}, bf16[3,96,1024]{2,1,0:T(8,128)(2,1)S(1)}, u32[]{:S(2)}, u32[]{:S(2)}) collective-permute-start(bf16[3,96,1024]{2,1,0:T(8,128)(2,1)S(1)} %pad_maximum_fusion), channel_id=1, source_target_pairs={{0,2},{1,3},{2,0},{3,1},{4,6},{5,7},{6,4},{7,5},{8,10},{9,11},{10,... | collective-permute-start | bytes 1769480 | tf_op jit(solution)/shard_map/ppermute | solution.py:143
  13.1 9.0 %all-to-all-done = bf16[8,48,512]{2,1,0:T(8,128)(2,1)S(1)} async-done(((bf16[8,48,512]{2,1,0:T(8,128)(2,1)}), bf16[8,48,512]{2,1,0:T(8,128)(2,1)S(1)}, u32[]{:S(2)}, u32[]{:S(2)}) %all-to-all-start) | async-done | bytes 393248 | tf_op jit(solution)/shard_map/all_to_all | solution.py:152
  22.1 4.3 %collective-permute-done.1.got_ref = bf16[3,96,1024]{2,1,0:T(8,128)(2,1)S(1)} collective-permute-done((bf16[3,96,1024]{2,1,0:T(8,128)(2,1)S(1)}, bf16[3,96,1024]{2,1,0:T(8,128)(2,1)S(1)}, u32[]{:S(2)}, u32[]{:S(2)}) %collective-permute-start.1) | collective-permute-done | bytes 589856 | tf_op jit(solution)/shard_map/ppermute | solution.py:143
  26.4 0.8 %copy-done = bf16[3,96,1024]{2,1,0:T(8,128)(2,1)} copy-done((bf16[3,96,1024]{2,1,0:T(8,128)(2,1)}, bf16[3,96,1024]{2,1,0:T(8,128)(2,1)S(1)}, u32[]{:S(2)}) %copy-start) | copy-done | bytes 589848
  27.2 0.1 copy-done.6
  27.3 3.1 %project.1 = (f32[384,384]{1,0:T(8,128)}, bf16[384,384]{1,0:T(8,128)(2,1)}) custom-call(s32[4]{0:T(128)} %pad_add_fusion.at_ref, bf16[384,512]{1,0:T(8,128)(2,1)} %bitcast.36, bf16[384,512]{1,0:T(8,128)(2,1)} %copy-done.6, bf16[96,2048]{1,0:T(8,128)(2,1)} %bitcast.41, bf16[96,2048]{1,0:T(8,128)(2,1)} %bitcast.42, bf16[3,96,1024]{2,1,0:T(8,128)(2,1)} %copy-done), custom_call_target="tpu_custom_call" | custom-call | tf_op jit(solution)/shard_map/project/pallas_call | solution.py:113
  30.4 1.5 %collective-permute-start.2 = (bf16[384,384]{1,0:T(8,128)(2,1)}, bf16[384,384]{1,0:T(8,128)(2,1)S(1)}, u32[]{:S(2)}, u32[]{:S(2)}) collective-permute-start(bf16[384,384]{1,0:T(8,128)(2,1)} %get-tuple-element.8), channel_id=1, source_target_pairs={{0,2},{1,3},{2,0},{3,1},{4,6},{5,7},{6,4},{7,5},{8,10},{9,11},{10,... | collective-permute-start | bytes 884744 | tf_op jit(solution)/shard_map/ppermute | solution.py:185
  31.9 0.9 %slice-done = bf16[1,96,1024]{2,1,0:T(8,128)(2,1)S(1)} async-done(((bf16[3,96,1024]{2,1,0:T(8,128)(2,1)}), bf16[1,96,1024]{2,1,0:T(8,128)(2,1)S(1)}, s32[]{:S(2)}) %slice-start) | async-done | bytes 196632 | tf_op jit(solution)/shard_map/slice | solution.py:166
  32.9 0.1 collective-permute-start.4
  33.0 5.3 %collective-permute-done.2.got_ref = bf16[384,384]{1,0:T(8,128)(2,1)S(1)} collective-permute-done((bf16[384,384]{1,0:T(8,128)(2,1)}, bf16[384,384]{1,0:T(8,128)(2,1)S(1)}, u32[]{:S(2)}, u32[]{:S(2)}) %collective-permute-start.2) | collective-permute-done | bytes 294944 | tf_op jit(solution)/shard_map/ppermute | solution.py:185
  38.2 0.7 %copy-done.7 = bf16[384,384]{1,0:T(8,128)(2,1)} copy-done((bf16[384,384]{1,0:T(8,128)(2,1)}, bf16[384,384]{1,0:T(8,128)(2,1)S(1)}, u32[]{:S(2)}) %copy-start.7) | copy-done | bytes 294936
  39.0 1.9 %hidden.1.mine_ref = bf16[192,384]{1,0:T(8,128)(2,1)} custom-call(f32[384,384]{1,0:T(8,128)} %get-tuple-element.7.full_ref, bf16[384,384]{1,0:T(8,128)(2,1)} %copy-done.7), custom_call_target="tpu_custom_call" | custom-call | tf_op jit(solution)/shard_map/hidden/pallas_call | solution.py:113
  40.9 1.6 %collective-permute-done.3.other_ref = bf16[192,384]{1,0:T(8,128)(2,1)S(1)} collective-permute-done((bf16[192,384]{1,0:T(8,128)(2,1)}, bf16[192,384]{1,0:T(8,128)(2,1)S(1)}, u32[]{:S(2)}, u32[]{:S(2)}) %collective-permute-start.3) | collective-permute-done | bytes 147488 | tf_op jit(solution)/shard_map/ppermute | solution.py:192
  42.5 0.6 copy-done.9
  43.1 2.5 %down.1 = bf16[384,512]{1,0:T(8,128)(2,1)} custom-call(s32[4]{0:T(128)} %pad_add_fusion.at_ref, bf16[192,384]{1,0:T(8,128)(2,1)} %hidden.1.mine_ref, bf16[192,384]{1,0:T(8,128)(2,1)} %copy-done.9, bf16[96,2048]{1,0:T(8,128)(2,1)} %bitcast.40, bf16[3,96,1024]{2,1,0:T(8,128)(2,1)} %copy-done, bf16[192,512]{1,0:T(8,128)(2,1)} %copy-done.8), custom_call_target="tpu_custom_call" | custom-call | tf_op jit(solution)/shard_map/down/pallas_call | solution.py:113
  45.6 5.4 %all-to-all-start.1 = ((bf16[8,48,512]{2,1,0:T(8,128)(2,1)}), bf16[8,48,512]{2,1,0:T(8,128)(2,1)S(1)}, u32[]{:S(2)}, u32[]{:S(2)}) async-start(bf16[8,48,512]{2,1,0:T(8,128)(2,1)} %bitcast.38), calls=%async_computation.1 | async-start | bytes 786432 | tf_op jit(solution)/shard_map/all_to_all | solution.py:195
  51.0 1.7 %gates.1.gates_ref = bf16[768,128]{1,0:T(8,128)(2,1)} custom-call(s32[2,128]{1,0:T(2,128)} %bitcast.45, f32[1,128]{1,0:T(1,128)} %bitcast.47, f32[2,128]{1,0:T(2,128)} %bitcast.46), custom_call_target="tpu_custom_call" | custom-call | tf_op jit(solution)/shard_map/gates/pallas_call | solution.py:113
  52.8 10.3 %all-to-all-done.1 = bf16[8,48,512]{2,1,0:T(8,128)(2,1)S(1)} async-done(((bf16[8,48,512]{2,1,0:T(8,128)(2,1)}), bf16[8,48,512]{2,1,0:T(8,128)(2,1)S(1)}, u32[]{:S(2)}, u32[]{:S(2)}) %all-to-all-start.1) | async-done | bytes 393248 | tf_op jit(solution)/shard_map/all_to_all | solution.py:195
  63.0 0.8 %copy-done.2 = bf16[8,48,512]{2,1,0:T(8,128)(2,1)} copy-done((bf16[8,48,512]{2,1,0:T(8,128)(2,1)}, bf16[8,48,512]{2,1,0:T(8,128)(2,1)S(1)}, u32[]{:S(2)}) %copy-start.2) | copy-done | bytes 393240
  63.8 2.1 %combine.1 = bf16[128,512]{1,0:T(8,128)(2,1)} custom-call(bf16[768,128]{1,0:T(8,128)(2,1)} %gates.1.gates_ref, bf16[384,512]{1,0:T(8,128)(2,1)} %bitcast.39), custom_call_target="tpu_custom_call" | custom-call | tf_op jit(solution)/shard_map/combine/pallas_call | solution.py:113
  (25 shorter events, 0.2 us)
Async XLA Ops:
  3.0 7.5 %copy-start.3 = (bf16[1,96,2048]{2,1,0:T(8,128)(2,1)S(1)}, bf16[1,96,2048]{2,1,0:T(8,128)(2,1)}, u32[]{:S(2)}) copy-start(bf16[1,96,2048]{2,1,0:T(8,128)(2,1)} %param.15) | copy-start | bytes 1179652
  3.0 7.5 %copy-start.5 = (bf16[1,2048,96]{1,2,0:T(8,128)(2,1)S(1)}, bf16[1,2048,96]{1,2,0:T(8,128)(2,1)}, u32[]{:S(2)}) copy-start(bf16[1,2048,96]{1,2,0:T(8,128)(2,1)} %param.14) | copy-start | bytes 1179652
  3.0 19.1 %all-to-all-start = ((bf16[8,48,512]{2,1,0:T(8,128)(2,1)}), bf16[8,48,512]{2,1,0:T(8,128)(2,1)S(1)}, u32[]{:S(2)}, u32[]{:S(2)}) async-start(bf16[8,48,512]{2,1,0:T(8,128)(2,1)} %bitcast.37), calls=%async_computation | async-start | bytes 786432 | tf_op jit(solution)/shard_map/all_to_all | solution.py:152
  10.4 1.0 %copy-start.4 = (bf16[1,2048,96]{1,2,0:T(8,128)(2,1)S(1)}, bf16[1,2048,96]{1,2,0:T(8,128)(2,1)}, u32[]{:S(2)}) copy-start(bf16[1,2048,96]{1,2,0:T(8,128)(2,1)} %param.13) | copy-start | bytes 1179652
  11.5 14.9 %collective-permute-start.1 = (bf16[3,96,1024]{2,1,0:T(8,128)(2,1)S(1)}, bf16[3,96,1024]{2,1,0:T(8,128)(2,1)S(1)}, u32[]{:S(2)}, u32[]{:S(2)}) collective-permute-start(bf16[3,96,1024]{2,1,0:T(8,128)(2,1)S(1)} %pad_maximum_fusion), channel_id=1, source_target_pairs={{0,2},{1,3},{2,0},{3,1},{4,6},{5,7},{6,4},{7,5},{8,10},{9,11},{10,... | collective-permute-start | bytes 1769480 | tf_op jit(solution)/shard_map/ppermute | solution.py:143
  22.1 4.3 %copy-start.1 = (bf16[8,48,512]{2,1,0:T(8,128)(2,1)}, bf16[8,48,512]{2,1,0:T(8,128)(2,1)S(1)}, u32[]{:S(2)}) copy-start(bf16[8,48,512]{2,1,0:T(8,128)(2,1)S(1)} %all-to-all-done) | copy-start | bytes 1179652
  22.1 4.3 %collective-permute-start = (bf16[384,512]{1,0:T(8,128)(2,1)S(1)}, bf16[384,512]{1,0:T(8,128)(2,1)S(1)}, u32[]{:S(2)}, u32[]{:S(2)}) collective-permute-start(bf16[384,512]{1,0:T(8,128)(2,1)S(1)} %bitcast.35), channel_id=1, source_target_pairs={{0,1},{1,0},{2,3},{3,2},{4,5},{5,4},{6,7},{7,6},{8,9},{9,8},{10,11... | collective-permute-start | bytes 1179656 | tf_op jit(solution)/shard_map/ppermute | solution.py:173
  26.4 0.8 %copy-start = (bf16[3,96,1024]{2,1,0:T(8,128)(2,1)}, bf16[3,96,1024]{2,1,0:T(8,128)(2,1)S(1)}, u32[]{:S(2)}) copy-start(bf16[3,96,1024]{2,1,0:T(8,128)(2,1)S(1)} %collective-permute-done.1.got_ref) | copy-start | bytes 1769476
  26.4 0.9 %copy-start.6 = (bf16[384,512]{1,0:T(8,128)(2,1)}, bf16[384,512]{1,0:T(8,128)(2,1)S(1)}, u32[]{:S(2)}) copy-start(bf16[384,512]{1,0:T(8,128)(2,1)S(1)} %collective-permute-done.other_ref) | copy-start | bytes 1179652
  30.4 7.8 %collective-permute-start.2 = (bf16[384,384]{1,0:T(8,128)(2,1)}, bf16[384,384]{1,0:T(8,128)(2,1)S(1)}, u32[]{:S(2)}, u32[]{:S(2)}) collective-permute-start(bf16[384,384]{1,0:T(8,128)(2,1)} %get-tuple-element.8), channel_id=1, source_target_pairs={{0,2},{1,3},{2,0},{3,1},{4,6},{5,7},{6,4},{7,5},{8,10},{9,11},{10,... | collective-permute-start | bytes 884744 | tf_op jit(solution)/shard_map/ppermute | solution.py:185
  31.9 0.9 %slice-start = ((bf16[3,96,1024]{2,1,0:T(8,128)(2,1)}), bf16[1,96,1024]{2,1,0:T(8,128)(2,1)S(1)}, s32[]{:S(2)}) async-start(bf16[3,96,1024]{2,1,0:T(8,128)(2,1)} %copy-done), calls=%async_computation.2 | async-start | bytes 393216 | tf_op jit(solution)/shard_map/slice | solution.py:166
  32.9 8.0 %collective-permute-start.4 = (bf16[192,512]{1,0:T(8,128)(2,1)S(1)}, bf16[192,512]{1,0:T(8,128)(2,1)S(1)}, u32[]{:S(2)}, u32[]{:S(2)}) collective-permute-start(bf16[192,512]{1,0:T(8,128)(2,1)S(1)} %pad_maximum_fusion.1), channel_id=1, source_target_pairs={{0,1},{1,0},{2,3},{3,2},{4,5},{5,4},{6,7},{7,6},{8,9},{9,8},{10,11... | collective-permute-start | bytes 589832 | tf_op jit(solution)/shard_map/ppermute | solution.py:162
  38.2 0.7 %copy-start.7 = (bf16[384,384]{1,0:T(8,128)(2,1)}, bf16[384,384]{1,0:T(8,128)(2,1)S(1)}, u32[]{:S(2)}) copy-start(bf16[384,384]{1,0:T(8,128)(2,1)S(1)} %collective-permute-done.2.got_ref) | copy-start | bytes 884740
  40.9 1.6 %collective-permute-start.3 = (bf16[192,384]{1,0:T(8,128)(2,1)}, bf16[192,384]{1,0:T(8,128)(2,1)S(1)}, u32[]{:S(2)}, u32[]{:S(2)}) collective-permute-start(bf16[192,384]{1,0:T(8,128)(2,1)} %hidden.1.mine_ref), channel_id=1, source_target_pairs={{0,1},{1,0},{2,3},{3,2},{4,5},{5,4},{6,7},{7,6},{8,9},{9,8},{10,11... | collective-permute-start | bytes 442376 | tf_op jit(solution)/shard_map/ppermute | solution.py:192
  40.9 1.6 %copy-start.8 = (bf16[192,512]{1,0:T(8,128)(2,1)}, bf16[192,512]{1,0:T(8,128)(2,1)S(1)}, u32[]{:S(2)}) copy-start(bf16[192,512]{1,0:T(8,128)(2,1)S(1)} %collective-permute-done.4.pair_ref) | copy-start | bytes 589828
  42.4 0.7 copy-start.9
  45.6 17.4 %all-to-all-start.1 = ((bf16[8,48,512]{2,1,0:T(8,128)(2,1)}), bf16[8,48,512]{2,1,0:T(8,128)(2,1)S(1)}, u32[]{:S(2)}, u32[]{:S(2)}) async-start(bf16[8,48,512]{2,1,0:T(8,128)(2,1)} %bitcast.38), calls=%async_computation.1 | async-start | bytes 786432 | tf_op jit(solution)/shard_map/all_to_all | solution.py:195
  63.0 0.8 %copy-start.2 = (bf16[8,48,512]{2,1,0:T(8,128)(2,1)}, bf16[8,48,512]{2,1,0:T(8,128)(2,1)S(1)}, u32[]{:S(2)}) copy-start(bf16[8,48,512]{2,1,0:T(8,128)(2,1)S(1)} %all-to-all-done.1) | copy-start | bytes 1179652

commit v2 on v1

--- a/solution.py
+++ b/solution.py
@@ -7,13 +7,17 @@
 from jax.experimental.pallas import tpu as pltpu
 from jax.sharding import PartitionSpec as P
 
+
 F32, BF16, I32 = jnp.float32, jnp.bfloat16, jnp.int32
 VM = pl.BlockSpec(memory_space=pltpu.VMEM)
-SM = pl.BlockSpec(memory_space=pltpu.SMEM)
 
 
 def dot(a, b, ca, cb):
     return lax.dot_general(a, b, (((ca,), (cb,)), ((), ())), preferred_element_type=F32)
+
+
+def columns(index, width):
+    return pl.ds(pl.multiple_of(index * width, width), width)
 
 
 def slot_tables(routes, experts, capacity):
@@ -39,11 +43,11 @@
     return spread, held
 
 
-def dispatch_kernel(experts, capacity, at_ref, tokens_ref, gain_ref, routes_ref, out_ref):
+def dispatch_kernel(experts, capacity, tokens_ref, gain_ref, routes_ref, out_ref):
     width = out_ref.shape[1]
     values = tokens_ref[...].astype(F32)
     scale = lax.rsqrt(jnp.mean(values * values, -1, keepdims=True) + 1e-06)
-    here = pl.ds(pl.multiple_of(at_ref[0] * width, width), width)
+    here = columns(lax.axis_index("tp"), width)
     normed = (tokens_ref[:, here].astype(F32) * scale * gain_ref[:, here]).astype(BF16)
     _, held = slot_tables(routes_ref[...], experts, capacity)
     picks = jnp.where(held, 1.0, 0.0).astype(BF16)
@@ -67,12 +71,11 @@
     out_ref[slots:] = jnp.where(held, dot(spread, low, 1, 0), 0.0).astype(BF16)
 
 
-def project_kernel(at_ref, mine_ref, other_ref, gate_ref, up_ref, got_ref, full_ref, send_ref):
+def project_kernel(mine_ref, other_ref, gate_ref, up_ref, got_ref, full_ref, send_ref):
     width = mine_ref.shape[1]
-    here = pl.ds(pl.multiple_of(at_ref[0] * width, width), width)
-    there = pl.ds(pl.multiple_of(at_ref[1] * width, width), width)
-    near = pl.ds(pl.multiple_of(at_ref[2] * width, width), width)
-    far = pl.ds(pl.multiple_of(at_ref[3] * width, width), width)
+    q = lax.axis_index("tp")
+    here, there = columns(q, width), columns(q ^ 1, width)
+    near, far = columns(q & 1, width), columns(1 - (q & 1), width)
     first = jnp.concatenate(
         [gate_ref[:, here], up_ref[:, here], got_ref[0, :, near], got_ref[1, :, near]], 0
     )
@@ -93,13 +96,13 @@
         out_ref[rows * half : rows * (half + 1)] = (gate / (1.0 + jnp.exp(-gate)) * up).astype(BF16)
 
 
-def down_kernel(at_ref, mine_ref, other_ref, down_ref, got_ref, pair_ref, out_ref):
+def down_kernel(mine_ref, other_ref, down_ref, got_ref, pair_ref, out_ref):
     width = out_ref.shape[1]
-    here = pl.ds(pl.multiple_of(at_ref[0] * width, width), width)
-    near = pl.ds(pl.multiple_of(at_ref[2] * width, width), width)
+    q = lax.axis_index("tp")
+    here, near = columns(q, width), columns(q & 1, width)
     hidden = jnp.concatenate([mine_ref[...], other_ref[...]], 0)
-    columns = jnp.concatenate([down_ref[:, here], got_ref[2, :, near], pair_ref[...]], 0)
-    out_ref[...] = dot(hidden, columns, 0, 0).astype(BF16)
+    weights = jnp.concatenate([down_ref[:, here], got_ref[2, :, near], pair_ref[...]], 0)
+    out_ref[...] = dot(hidden, weights, 0, 0).astype(BF16)
 
 
 def combine_kernel(gates_ref, back_ref, out_ref):
@@ -109,14 +112,14 @@
     out_ref[...] = total.astype(BF16)
 
 
-def call(kernel, shapes, scalars, arrays, name):
+def call(kernel, shapes, arrays):
     return pl.pallas_call(
         kernel,
         out_shape=shapes,
-        in_specs=[SM] * len(scalars) + [VM] * len(arrays),
+        in_specs=[VM] * len(arrays),
         out_specs=jax.tree.map(lambda _: VM, shapes),
-        name=name,
-    )(*scalars, *arrays)
+        compiler_params=pltpu.CompilerParams(vmem_limit_bytes=16 * 2**20),
+    )(*arrays)
 
 
 def body(tokens, norm_gain, routes, group_prob, expert_logits, gate_weight, up_weight, down_matrix):
@@ -131,12 +134,11 @@
     shape = jax.ShapeDtypeStruct
 
     q = lax.axis_index("tp").astype(I32)
-    at = jnp.stack([q, q ^ 1, q % 2, 1 - q % 2])
     near = [(i, i ^ 1) for i in range(tp)]
     far = [(i, i ^ 2) for i in range(tp)]
 
     gate, up, down = gate_weight[0].T, up_weight[0].T, down_matrix[0]
-    away = (1 - q // 2) * (2 * width)
+    away = (1 - (q >> 1)) * (2 * width)
     packed = jnp.stack(
         [lax.dynamic_slice_in_dim(w, away, 2 * width, 1) for w in (gate, up, down)]
     )
@@ -145,9 +147,7 @@
     outgoing = call(
         functools.partial(dispatch_kernel, experts, capacity),
         shape((slots, width), BF16),
-        [at],
         [tokens, norm_gain[None], routes.T],
-        "dispatch",
     )
     mine = lax.all_to_all(
         outgoing.reshape(ep, slots // ep, width), "ep", split_axis=0, concat_axis=0, tiled=True
@@ -155,15 +155,13 @@
     gates = call(
         functools.partial(gates_kernel, experts, capacity),
         shape((2 * slots, tok_rows), BF16),
-        [],
         [routes.T, group_prob[None], expert_logits.T],
-        "gates",
     )
     pair = lax.ppermute(
         jnp.concatenate(
             [
-                lax.dynamic_slice_in_dim(down, at[1] * width, width, 1),
-                lax.dynamic_slice_in_dim(got[2], at[3] * width, width, 1),
+                lax.dynamic_slice_in_dim(down, (q ^ 1) * width, width, 1),
+                lax.dynamic_slice_in_dim(got[2], (1 - (q & 1)) * width, width, 1),
             ],
             0,
         ),
@@ -174,28 +172,20 @@
     full, send = call(
         project_kernel,
         (shape((4 * block, slots), F32), shape((4 * block, slots), BF16)),
-        [at],
         [mine, other, gate, up, got],
-        "project",
     )
     hidden = call(
-        hidden_kernel,
-        shape((2 * block, slots), BF16),
-        [],
-        [full, lax.ppermute(send, "tp", far)],
-        "hidden",
+        hidden_kernel, shape((2 * block, slots), BF16), [full, lax.ppermute(send, "tp", far)]
     )
     summed = call(
         down_kernel,
         shape((slots, width), BF16),
-        [at],
         [hidden, lax.ppermute(hidden, "tp", near), down, got, pair],
-        "down",
     )
     back = lax.all_to_all(
         summed.reshape(ep, slots // ep, width), "ep", split_axis=0, concat_axis=0, tiled=True
     ).reshape(slots, width)
-    return call(combine_kernel, shape((tok_rows, width), BF16), [], [gates, back], "combine")
+    return call(combine_kernel, shape((tok_rows, width), BF16), [gates, back])
 
 
 def solution(mesh):

time: 66.4 us -> 57.9 us (0.87)
  Pallas kernels: 13.6 us -> 4.46 us
  waiting for transfers between devices: 30.4 us -> 31.8 us
  local copies, waits for them, and re-layouts: 4.97 us -> 4.12 us
    pallas_call x6, Pallas kernels: 13.6 us -> 4.46 us  [call(): pl.pallas_call(kernel, out_shape=shapes, in_specs=[VM] * len(arrays), out...]
    ppermute x1, waiting for transfers between devices: 4.28 us -> 5.24 us  [body(): got = lax.ppermute(packed, 'tp', far)]
    slice x2 -> x1, local copies, waits for them, and re-layouts: 0.92 us -> 0.01 us  [body(): got[2]]
    another operation x1, other arithmetic: 0.07 us -> 0.89 us  [body(): jnp.stack([lax.dynamic_slice_in_dim(w, away, 2 * width, 1) for w in (gate...]
    all_to_all x1, waiting for transfers between devices: 9.02 us -> 8.26 us  [body(): lax.all_to_all(outgoing.reshape(ep, slots // ep, width), 'ep', split_axis...]
    all_to_all x1, waiting for transfers between devices: 10.3 us -> 10.9 us  [body(): lax.all_to_all(summed.reshape(ep, slots // ep, width), 'ep', split_axis=0...]
    ppermute x1, waiting for transfers between devices: 5.28 us -> 5.97 us  [body(): lax.ppermute(send, 'tp', far)]
    unnamed x20 -> x16, local copies, waits for them, and re-layouts: 3.99 us -> 4.03 us
  transfers between devices with their start and end apart: 7 -> 7, of which waited for: 5 -> 5; matrix products, arithmetic and copies ran while one was open for 0% -> 2% of each run, Pallas kernels for 6% -> 1%
where the time goes in v2:
time: 57.9 us; the launch traced here: 57.4 us
  waiting for transfers between devices  31.8 us (55%)
  starting transfers between devices  16.1 us (28%)
  Pallas kernels  4.46 us (8%)
  local copies, waits for them, and re-layouts  4.12 us (7%)
  other arithmetic  0.91 us (2%)
    all_to_all x1, waiting for transfers between devices, body(): lax.all_to_all(summed.reshape(ep, slots // ep, width), 'ep', split_axis=0...  10.9 us
    all_to_all x1, waiting for transfers between devices, body(): lax.all_to_all(outgoing.reshape(ep, slots // ep, width), 'ep', split_axis...  8.26 us
    all_to_all x1, starting transfers between devices, body(): lax.all_to_all(outgoing.reshape(ep, slots // ep, width), 'ep', split_axis...  7.44 us
    ppermute x1, waiting for transfers between devices, body(): lax.ppermute(send, 'tp', far)  5.97 us
    all_to_all x1, starting transfers between devices, body(): lax.all_to_all(summed.reshape(ep, slots // ep, width), 'ep', split_axis=0...  5.43 us
    ppermute x1, waiting for transfers between devices, body(): got = lax.ppermute(packed, 'tp', far)  5.24 us
    pallas_call x6, Pallas kernels, call(): pl.pallas_call(kernel, out_shape=shapes, in_specs=[VM] * len(arrays), out...  4.46 us
    unnamed x16, local copies, waits for them, and re-layouts  4.03 us
  transfers between devices with their start and end apart: 7, of which 5 were waited for; matrix products, arithmetic and copies ran while one was open for 2% of the time, Pallas kernels for 1%

profile of v2, /device:TPU:0, one launch (start us, length us, event | category | flops | bytes accessed | tf_op | source)
XLA Modules:
  0.0 57.4 jit_solution(3730696906910603765)
XLA Ops:
  0.0 0.7 %copy-done.5 = s32[128,2]{0,1:T(2,128)S(1)} copy-done((s32[128,2]{0,1:T(2,128)S(1)}, s32[128,2]{0,1:T(2,128)}, u32[]{:S(2)}) %copy-start.5) | copy-done | bytes 1048
  0.7 1.0 %copy-done.3 = bf16[128,2048]{1,0:T(8,128)(2,1)S(1)} copy-done((bf16[128,2048]{1,0:T(8,128)(2,1)S(1)}, bf16[128,2048]{1,0:T(8,128)(2,1)}, u32[]{:S(2)}) %copy-start.3) | copy-done | bytes 524312
  1.7 0.7 %copy-done.4 = f32[2048]{0:T(1024)S(1)} copy-done((f32[2048]{0:T(1024)S(1)}, f32[2048]{0:T(1024)}, u32[]{:S(2)}) %copy-start.4) | copy-done | bytes 8216
  2.4 1.3 %shard_map.83 = bf16[384,512]{1,0:T(8,128)(2,1)} custom-call(bf16[128,2048]{1,0:T(8,128)(2,1)S(1)} %copy-done.3, f32[1,2048]{1,0:T(1,128)S(1)} %bitcast.37, s32[2,128]{1,0:T(2,128)S(1)} %bitcast.38), custom_call_target="tpu_custom_call" | custom-call | tf_op jit(solution)/shard_map/pallas_call | solution.py:116
  3.7 7.4 %all-to-all-start = ((bf16[8,48,512]{2,1,0:T(8,128)(2,1)}), bf16[8,48,512]{2,1,0:T(8,128)(2,1)S(1)}, u32[]{:S(2)}, u32[]{:S(2)}) async-start(bf16[8,48,512]{2,1,0:T(8,128)(2,1)} %bitcast.4), calls=%async_computation | async-start | bytes 786432 | tf_op jit(solution)/shard_map/all_to_all | solution.py:152
  11.2 0.9 %copy-done.1 = bf16[1,2048,96]{1,2,0:T(8,128)(2,1)S(1)} copy-done((bf16[1,2048,96]{1,2,0:T(8,128)(2,1)S(1)}, bf16[1,2048,96]{1,2,0:T(8,128)(2,1)}, u32[]{:S(2)}) %copy-start.1) | copy-done | bytes 393240
  12.2 0.9 %pad_maximum_fusion = bf16[3,96,1024]{2,1,0:T(8,128)(2,1)} fusion(bf16[1,96,1024]{2,1,0:T(8,128)(2,1)S(1)} %constant_dynamic-slice_fusion, bf16[1,96,1024]{2,1,0:T(8,128)(2,1)S(1)} %get-tuple-element.9, bf16[1,96,1024]{2,1,0:T(8,128)(2,1)S(1)} %get-tuple-element.10), kind=kLoop, calls=%fused_computation | loop fusion | flops 589824 | bytes 1179648 | tf_op jit(solution)/shard_map/stack | solution.py:142
  13.1 1.5 %collective-permute-start.1 = (bf16[3,96,1024]{2,1,0:T(8,128)(2,1)}, bf16[3,96,1024]{2,1,0:T(8,128)(2,1)S(1)}, u32[]{:S(2)}, u32[]{:S(2)}) collective-permute-start(bf16[3,96,1024]{2,1,0:T(8,128)(2,1)} %pad_maximum_fusion), channel_id=1, source_target_pairs={{0,2},{1,3},{2,0},{3,1},{4,6},{5,7},{6,4},{7,5},{8,10},{9,11},{10,... | collective-permute-start | bytes 1769480 | tf_op jit(solution)/shard_map/ppermute | solution.py:145
  14.5 8.3 %all-to-all-done = bf16[8,48,512]{2,1,0:T(8,128)(2,1)S(1)} async-done(((bf16[8,48,512]{2,1,0:T(8,128)(2,1)}), bf16[8,48,512]{2,1,0:T(8,128)(2,1)S(1)}, u32[]{:S(2)}, u32[]{:S(2)}) %all-to-all-start) | async-done | bytes 393248 | tf_op jit(solution)/shard_map/all_to_all | solution.py:152
  22.8 5.2 %collective-permute-done.1.got_ref = bf16[3,96,1024]{2,1,0:T(8,128)(2,1)S(1)} collective-permute-done((bf16[3,96,1024]{2,1,0:T(8,128)(2,1)}, bf16[3,96,1024]{2,1,0:T(8,128)(2,1)S(1)}, u32[]{:S(2)}, u32[]{:S(2)}) %collective-permute-start.1) | collective-permute-done | bytes 589856 | tf_op jit(solution)/shard_map/ppermute | solution.py:145
  28.1 0.6 %shard_map.84 = (f32[384,384]{1,0:T(8,128)S(1)}, bf16[384,384]{1,0:T(8,128)(2,1)S(1)}) custom-call(bf16[384,512]{1,0:T(8,128)(2,1)S(1)} %bitcast.33, bf16[384,512]{1,0:T(8,128)(2,1)S(1)} %collective-permute-done.other_ref, bf16[96,2048]{1,0:T(8,128)(2,1)S(1)} %bitcast.35, bf16[96,2048]{1,0:T(8,128)(2,1)S(1)} %bitcast.36, ...), custom_call_target="tpu_custom_call" | custom-call | tf_op jit(solution)/shard_map/pallas_call | solution.py:116
  28.7 1.6 %collective-permute-start.2 = (bf16[384,384]{1,0:T(8,128)(2,1)S(1)}, bf16[384,384]{1,0:T(8,128)(2,1)S(1)}, u32[]{:S(2)}, u32[]{:S(2)}) collective-permute-start(bf16[384,384]{1,0:T(8,128)(2,1)S(1)} %get-tuple-element.8), channel_id=1, source_target_pairs={{0,2},{1,3},{2,0},{3,1},{4,6},{5,7},{6,4},{7,5},{8,10},{9,11},{10,... | collective-permute-start | bytes 884744 | tf_op jit(solution)/shard_map/ppermute | solution.py:178
  30.3 0.1 collective-permute-start.4
  30.4 6.0 %collective-permute-done.2.got_ref = bf16[384,384]{1,0:T(8,128)(2,1)S(1)} collective-permute-done((bf16[384,384]{1,0:T(8,128)(2,1)S(1)}, bf16[384,384]{1,0:T(8,128)(2,1)S(1)}, u32[]{:S(2)}, u32[]{:S(2)}) %collective-permute-start.2) | collective-permute-done | bytes 294944 | tf_op jit(solution)/shard_map/ppermute | solution.py:178
  36.3 0.1 shard_map.85.mine_ref
  36.5 0.1 collective-permute-start.3
  36.6 1.3 %collective-permute-done.3.other_ref = bf16[192,384]{1,0:T(8,128)(2,1)S(1)} collective-permute-done((bf16[192,384]{1,0:T(8,128)(2,1)S(1)}, bf16[192,384]{1,0:T(8,128)(2,1)S(1)}, u32[]{:S(2)}, u32[]{:S(2)}) %collective-permute-start.3) | collective-permute-done | bytes 147488 | tf_op jit(solution)/shard_map/ppermute | solution.py:183
  37.9 1.1 %shard_map.86 = bf16[384,512]{1,0:T(8,128)(2,1)} custom-call(bf16[192,384]{1,0:T(8,128)(2,1)S(1)} %shard_map.85.mine_ref, bf16[192,384]{1,0:T(8,128)(2,1)S(1)} %collective-permute-done.3.other_ref, bf16[96,2048]{1,0:T(8,128)(2,1)S(1)} %bitcast.34, bf16[3,96,1024]{2,1,0:T(8,128)(2,1)S(1)} %collective-permute-done.1.got_ref, ...), custom_call_target="tpu_custom_call" | custom-call | tf_op jit(solution)/shard_map/pallas_call | solution.py:116
  39.0 5.4 %all-to-all-start.1 = ((bf16[8,48,512]{2,1,0:T(8,128)(2,1)}), bf16[8,48,512]{2,1,0:T(8,128)(2,1)S(1)}, u32[]{:S(2)}, u32[]{:S(2)}) async-start(bf16[8,48,512]{2,1,0:T(8,128)(2,1)} %bitcast.19), calls=%async_computation.1 | async-start | bytes 786432 | tf_op jit(solution)/shard_map/all_to_all | solution.py:185
  44.5 0.0 copy-start.7
  44.5 0.7 %copy-done.6 = f32[128,2]{0,1:T(2,128)S(1)} copy-done((f32[128,2]{0,1:T(2,128)S(1)}, f32[128,2]{0,1:T(2,128)}, u32[]{:S(2)}) %copy-start.6) | copy-done | bytes 1048
  45.2 0.4 shard_map.82.gates_ref
  45.5 10.9 %all-to-all-done.1 = bf16[8,48,512]{2,1,0:T(8,128)(2,1)S(1)} async-done(((bf16[8,48,512]{2,1,0:T(8,128)(2,1)}), bf16[8,48,512]{2,1,0:T(8,128)(2,1)S(1)}, u32[]{:S(2)}, u32[]{:S(2)}) %all-to-all-start.1) | async-done | bytes 393248 | tf_op jit(solution)/shard_map/all_to_all | solution.py:185
  56.5 1.0 %shard_map.87 = bf16[128,512]{1,0:T(8,128)(2,1)} custom-call(bf16[768,128]{1,0:T(8,128)(2,1)S(1)} %shard_map.82.gates_ref, bf16[384,512]{1,0:T(8,128)(2,1)S(1)} %bitcast.31), custom_call_target="tpu_custom_call" | custom-call | tf_op jit(solution)/shard_map/pallas_call | solution.py:116
  (19 shorter events, 0.1 us)
Async XLA Ops:
  0.0 0.7 %copy-start.5 = (s32[128,2]{0,1:T(2,128)S(1)}, s32[128,2]{0,1:T(2,128)}, u32[]{:S(2)}) copy-start(s32[128,2]{0,1:T(2,128)} %param.10) | copy-start | bytes 3076
  0.7 1.0 %copy-start.3 = (bf16[128,2048]{1,0:T(8,128)(2,1)S(1)}, bf16[128,2048]{1,0:T(8,128)(2,1)}, u32[]{:S(2)}) copy-start(bf16[128,2048]{1,0:T(8,128)(2,1)} %tokens_ref.1) | copy-start | bytes 1572868
  1.7 0.7 %copy-start.4 = (f32[2048]{0:T(1024)S(1)}, f32[2048]{0:T(1024)}, u32[]{:S(2)}) copy-start(f32[2048]{0:T(1024)} %param.9) | copy-start | bytes 24580
  3.7 7.5 %copy-start = (bf16[1,96,2048]{2,1,0:T(8,128)(2,1)S(1)}, bf16[1,96,2048]{2,1,0:T(8,128)(2,1)}, u32[]{:S(2)}) copy-start(bf16[1,96,2048]{2,1,0:T(8,128)(2,1)} %param.15) | copy-start | bytes 1179652
  3.7 7.5 %copy-start.2 = (bf16[1,2048,96]{1,2,0:T(8,128)(2,1)S(1)}, bf16[1,2048,96]{1,2,0:T(8,128)(2,1)}, u32[]{:S(2)}) copy-start(bf16[1,2048,96]{1,2,0:T(8,128)(2,1)} %param.14) | copy-start | bytes 1179652
  3.7 19.1 %all-to-all-start = ((bf16[8,48,512]{2,1,0:T(8,128)(2,1)}), bf16[8,48,512]{2,1,0:T(8,128)(2,1)S(1)}, u32[]{:S(2)}, u32[]{:S(2)}) async-start(bf16[8,48,512]{2,1,0:T(8,128)(2,1)} %bitcast.4), calls=%async_computation | async-start | bytes 786432 | tf_op jit(solution)/shard_map/all_to_all | solution.py:152
  11.1 1.0 %copy-start.1 = (bf16[1,2048,96]{1,2,0:T(8,128)(2,1)S(1)}, bf16[1,2048,96]{1,2,0:T(8,128)(2,1)}, u32[]{:S(2)}) copy-start(bf16[1,2048,96]{1,2,0:T(8,128)(2,1)} %param.13) | copy-start | bytes 1179652
  13.1 15.0 %collective-permute-start.1 = (bf16[3,96,1024]{2,1,0:T(8,128)(2,1)}, bf16[3,96,1024]{2,1,0:T(8,128)(2,1)S(1)}, u32[]{:S(2)}, u32[]{:S(2)}) collective-permute-start(bf16[3,96,1024]{2,1,0:T(8,128)(2,1)} %pad_maximum_fusion), channel_id=1, source_target_pairs={{0,2},{1,3},{2,0},{3,1},{4,6},{5,7},{6,4},{7,5},{8,10},{9,11},{10,... | collective-permute-start | bytes 1769480 | tf_op jit(solution)/shard_map/ppermute | solution.py:145
  22.8 5.2 %collective-permute-start = (bf16[384,512]{1,0:T(8,128)(2,1)S(1)}, bf16[384,512]{1,0:T(8,128)(2,1)S(1)}, u32[]{:S(2)}, u32[]{:S(2)}) collective-permute-start(bf16[384,512]{1,0:T(8,128)(2,1)S(1)} %bitcast.32), channel_id=1, source_target_pairs={{0,1},{1,0},{2,3},{3,2},{4,5},{5,4},{6,7},{7,6},{8,9},{9,8},{10,11... | collective-permute-start | bytes 1179656 | tf_op jit(solution)/shard_map/ppermute | solution.py:171
  28.7 7.7 %collective-permute-start.2 = (bf16[384,384]{1,0:T(8,128)(2,1)S(1)}, bf16[384,384]{1,0:T(8,128)(2,1)S(1)}, u32[]{:S(2)}, u32[]{:S(2)}) collective-permute-start(bf16[384,384]{1,0:T(8,128)(2,1)S(1)} %get-tuple-element.8), channel_id=1, source_target_pairs={{0,2},{1,3},{2,0},{3,1},{4,6},{5,7},{6,4},{7,5},{8,10},{9,11},{10,... | collective-permute-start | bytes 884744 | tf_op jit(solution)/shard_map/ppermute | solution.py:178
  30.3 6.3 %collective-permute-start.4 = (bf16[192,512]{1,0:T(8,128)(2,1)S(1)}, bf16[192,512]{1,0:T(8,128)(2,1)S(1)}, u32[]{:S(2)}, u32[]{:S(2)}) collective-permute-start(bf16[192,512]{1,0:T(8,128)(2,1)S(1)} %pad_maximum_fusion.1), channel_id=1, source_target_pairs={{0,1},{1,0},{2,3},{3,2},{4,5},{5,4},{6,7},{7,6},{8,9},{9,8},{10,11... | collective-permute-start | bytes 589832 | tf_op jit(solution)/shard_map/ppermute | solution.py:160
  36.5 1.4 %collective-permute-start.3 = (bf16[192,384]{1,0:T(8,128)(2,1)S(1)}, bf16[192,384]{1,0:T(8,128)(2,1)S(1)}, u32[]{:S(2)}, u32[]{:S(2)}) collective-permute-start(bf16[192,384]{1,0:T(8,128)(2,1)S(1)} %shard_map.85.mine_ref), channel_id=1, source_target_pairs={{0,1},{1,0},{2,3},{3,2},{4,5},{5,4},{6,7},{7,6},{8,9},{9,8},{10,11... | collective-permute-start | bytes 442376 | tf_op jit(solution)/shard_map/ppermute | solution.py:183
  39.0 17.4 %all-to-all-start.1 = ((bf16[8,48,512]{2,1,0:T(8,128)(2,1)}), bf16[8,48,512]{2,1,0:T(8,128)(2,1)S(1)}, u32[]{:S(2)}, u32[]{:S(2)}) async-start(bf16[8,48,512]{2,1,0:T(8,128)(2,1)} %bitcast.19), calls=%async_computation.1 | async-start | bytes 786432 | tf_op jit(solution)/shard_map/all_to_all | solution.py:185
  44.5 0.7 %copy-start.6 = (f32[128,2]{0,1:T(2,128)S(1)}, f32[128,2]{0,1:T(2,128)}, u32[]{:S(2)}) copy-start(f32[128,2]{0,1:T(2,128)} %param.12) | copy-start | bytes 3076
  44.5 0.7 %copy-start.7 = (f32[128]{0:T(128)S(1)}, f32[128]{0:T(128)}, u32[]{:S(2)}) copy-start(f32[128]{0:T(128)} %param.11) | copy-start | bytes 1540

commit v3 on v2

v3 whole, which is shorter than its diff:
```python
import functools

import jax
import jax.numpy as jnp
from jax import lax
from jax.experimental import pallas as pl
from jax.experimental.pallas import tpu as pltpu
from jax.sharding import PartitionSpec as P


F32, BF16, I32 = jnp.float32, jnp.bfloat16, jnp.int32
VM = pl.BlockSpec(memory_space=pltpu.VMEM)
HBM = pl.BlockSpec(memory_space=pltpu.HBM)
PARTS = 1


def dot(a, b, ca, cb):
    return lax.dot_general(a, b, (((ca,), (cb,)), ((), ())), preferred_element_type=F32)


def columns(index, width):
    return pl.ds(pl.multiple_of(index * width, width), width)


def chunks(count):
    first = -(-count // 16) * 8
    if PARTS == 1 or first >= count:
        return [(0, count)]
    return [(0, first), (first, count - first)]


def places(routes, experts):
    top, count = routes.shape
    expert_of = lax.broadcasted_iota(I32, (experts, count), 0)
    named = routes[0:1] == expert_of
    for k in range(1, top):
        named = named | (routes[k : k + 1] == expert_of)
    ahead = lax.broadcasted_iota(I32, (count, count), 0) < lax.broadcasted_iota(
        I32, (count, count), 1
    )
    ones = jnp.where(named, 1.0, 0.0).astype(BF16)
    earlier = dot(ones, jnp.where(ahead, 1.0, 0.0).astype(BF16), 1, 0)
    return jnp.where(named, earlier, -1.0).astype(BF16)


def holders(place, base, length):
    experts = place.shape[0]
    rows = experts * length
    inside = lax.broadcasted_iota(I32, (rows, experts), 0) - length * lax.broadcasted_iota(
        I32, (rows, experts), 1
    )
    owned = (inside >= 0) & (inside < length)
    spread = jnp.where(owned, 1.0, 0.0).astype(BF16)
    slot = jnp.sum(jnp.where(owned, inside, 0), 1, keepdims=True) + base
    return spread, dot(spread, place, 1, 0) == slot.astype(F32)


def pack_kernel(gate_ref, up_ref, down_ref, away_ref, away_down_ref, keep_ref, sems):
    width = away_ref.shape[2]
    row = lax.axis_index("tp") >> 1
    here, there = columns(row, width), columns(1 - row, width)
    copies = [
        pltpu.make_async_copy(gate_ref.at[:, there], away_ref.at[0], sems.at[0]),
        pltpu.make_async_copy(up_ref.at[:, there], away_ref.at[1], sems.at[1]),
        pltpu.make_async_copy(down_ref.at[:, there], away_down_ref, sems.at[2]),
        pltpu.make_async_copy(gate_ref.at[:, here], keep_ref.at[0], sems.at[3]),
        pltpu.make_async_copy(up_ref.at[:, here], keep_ref.at[1], sems.at[4]),
        pltpu.make_async_copy(down_ref.at[:, here], keep_ref.at[2], sems.at[5]),
    ]
    for copy in copies:
        copy.start()
    for copy in copies:
        copy.wait()


def dispatch_kernel(experts, half, tokens_ref, gain_ref, routes_ref, *out_refs):
    width = out_refs[0].shape[1]
    q = lax.axis_index("tp")
    values = tokens_ref[...].astype(F32)
    scale = lax.rsqrt(jnp.mean(values * values, -1, keepdims=True) + 1e-06)
    here = columns(q >> 1, width)
    normed = (tokens_ref[:, here].astype(F32) * scale * gain_ref[:, here]).astype(BF16)
    place = places(routes_ref[...], experts)
    for (first, length), out_ref in zip(chunks(half), out_refs):
        _, held = holders(place, (q & 1) * half + first, length)
        out_ref[...] = dot(jnp.where(held, 1.0, 0.0).astype(BF16), normed, 1, 0).astype(BF16)


def gates_kernel(experts, half, routes_ref, prob_ref, logits_ref, *out_refs):
    routes, logits = routes_ref[...], logits_ref[...]
    top, count = routes.shape
    powers = jnp.exp(logits - jnp.max(logits, 0, keepdims=True))
    weights = prob_ref[...] * (powers / jnp.sum(powers, 0, keepdims=True))
    place = places(routes, experts)
    expert_of = lax.broadcasted_iota(I32, (experts, count), 0)
    by_expert = jnp.zeros((experts, count), F32)
    for k in range(top):
        by_expert = by_expert + jnp.where(routes[k : k + 1] == expert_of, weights[k : k + 1], 0.0)
    high = by_expert.astype(BF16)
    low = (by_expert - high.astype(F32)).astype(BF16)
    for (first, length), out_ref in zip(chunks(half), out_refs):
        spread, held = holders(place, (lax.axis_index("tp") & 1) * half + first, length)
        rows = experts * length
        out_ref[0:rows] = jnp.where(held, dot(spread, high, 1, 0), 0.0).astype(BF16)
        out_ref[rows:] = jnp.where(held, dot(spread, low, 1, 0), 0.0).astype(BF16)


def ordered(row, own, far):
    return [jnp.where(row == 0, own, far), jnp.where(row == 0, far, own)]


def project_kernel(mine_ref, keep_ref, far_ref, near_ref, near_far_ref, full_ref, send_ref):
    row = lax.axis_index("tp") >> 1
    pieces = []
    for i in range(2):
        pieces += ordered(row, keep_ref[i], far_ref[i])
        pieces += ordered(row, near_ref[i], near_far_ref[i])
    total = dot(mine_ref[...], jnp.concatenate(pieces, 0), 1, 1)
    full_ref[...] = total
    send_ref[...] = total.astype(BF16)


def expert_kernel(full_ref, got_ref, keep_ref, far_ref, near_ref, near_far_ref, out_ref):
    row = lax.axis_index("tp") >> 1
    width = full_ref.shape[1] // 2
    gate = full_ref[:, :width] + got_ref[:, :width].astype(F32)
    up = full_ref[:, width:] + got_ref[:, width:].astype(F32)
    hidden = (gate / (1.0 + jnp.exp(-gate)) * up).astype(BF16)
    down = ordered(row, keep_ref[2], far_ref[...]) + ordered(row, near_ref[2], near_far_ref[...])
    out_ref[...] = dot(hidden, jnp.concatenate(down, 0), 1, 0).astype(BF16)


def combine_kernel(parts, *refs):
    gates, backs, (own_ref, send_ref) = refs[:parts], refs[parts : 2 * parts], refs[2 * parts :]
    width = own_ref.shape[1]
    column = lax.axis_index("tp") & 1

    def total(at):
        result = None
        for gate_ref, back_ref in zip(gates, backs):
            rows = back_ref.shape[0]
            back = back_ref[:, at]
            part = dot(gate_ref[0:rows], back, 0, 0) + dot(gate_ref[rows:], back, 0, 0)
            result = part if result is None else result + part
        return result

    send_ref[...] = total(columns(1 - column, width)).astype(BF16)
    own_ref[...] = total(columns(column, width))


def call(kernel, shapes, arrays, specs=None, scratch=()):
    return pl.pallas_call(
        kernel,
        out_shape=shapes,
        in_specs=[VM] * len(arrays) if specs is None else specs,
        out_specs=jax.tree.map(lambda _: VM, shapes),
        scratch_shapes=scratch,
        compiler_params=pltpu.CompilerParams(vmem_limit_bytes=16 * 2**20),
    )(*arrays)


def body(tokens, norm_gain, routes, group_prob, expert_logits, gate_weight, up_weight, down_matrix):
    tok_rows, model_width = tokens.shape
    top = routes.shape[1]
    local, _, block = gate_weight.shape
    ep, tp = lax.axis_size("ep"), lax.axis_size("tp")
    experts = local * ep
    capacity = 3 * top * tok_rows // (2 * experts)
    half = -(-capacity // 2)
    width = model_width // 2
    parts = chunks(half)

    def shape(*dims, dtype=BF16):
        return jax.ShapeDtypeStruct(dims, dtype)

    near = [(i, i ^ 1) for i in range(tp)]
    far = [(i, i ^ 2) for i in range(tp)]

    def exchange(x, length):
        blocks = x.reshape(ep, local * length, width)
        return lax.all_to_all(blocks, "ep", split_axis=0, concat_axis=0, tiled=True).reshape(
            x.shape
        )

    away, away_down, keep = call(
        pack_kernel,
        (shape(2, block, width), shape(block, width), shape(3, block, width)),
        [gate_weight[0].T, up_weight[0].T, down_matrix[0]],
        [HBM] * 3,
        [pltpu.SemaphoreType.DMA((6,))],
    )
    got = lax.ppermute(away, "tp", far)
    got_down = lax.ppermute(away_down, "tp", far)
    near_keep = lax.ppermute(keep, "tp", near)
    near_got = lax.ppermute(got, "tp", near)
    near_got_down = lax.ppermute(got_down, "tp", near)

    outgoing = call(
        functools.partial(dispatch_kernel, experts, half),
        tuple(shape(experts * n, width) for _, n in parts),
        [tokens, norm_gain[None], routes.T],
    )
    gates = call(
        functools.partial(gates_kernel, experts, half),
        tuple(shape(2 * experts * n, tok_rows) for _, n in parts),
        [routes.T, group_prob[None], expert_logits.T],
    )
    arrived, projected, backs = [], [], []
    for i, (_, n) in enumerate(parts):
        arrived.append(exchange(outgoing[i], n))
    for i, (_, n) in enumerate(parts):
        full, send = call(
            project_kernel,
            (shape(experts * n, 8 * block, dtype=F32), shape(experts * n, 8 * block)),
            [arrived[i], keep, got, near_keep, near_got],
        )
        projected.append((full, lax.ppermute(send, "tp", far)))
    for i, (_, n) in enumerate(parts):
        summed = call(
            expert_kernel,
            shape(experts * n, width),
            [*projected[i], keep, got_down, near_keep, near_got_down],
        )
        backs.append(exchange(summed, n))
    own, send = call(
        functools.partial(combine_kernel, len(parts)),
        (shape(tok_rows, width // 2, dtype=F32), shape(tok_rows, width // 2)),
        [*gates, *backs],
    )
    return (own + lax.ppermute(send, "tp", near).astype(F32)).astype(BF16)


def solution(mesh):
    return jax.shard_map(
        body,
        mesh=mesh,
        in_specs=(
            P("ep", None),
            P(),
            P("ep", None),
            P("ep"),
            P("ep", None),
            P("ep", None, "tp"),
            P("ep", None, "tp"),
            P("ep", "tp", None),
        ),
        out_specs=P("ep", "tp"),
        check_vma=False,
    )
```

time: 57.9 us -> 53 us (0.915)
  waiting for transfers between devices: 31.8 us -> 26.8 us
  starting transfers between devices: 16.1 us -> 16.8 us
    ppermute x5 -> x7, waiting for transfers between devices: 12.6 us -> 8.85 us  [the longest x1 4.71 us: body(): projected.append((full, lax.ppermute(send, 'tp', far)))]
    ppermute x5 -> x7, starting transfers between devices: 3.19 us -> 5.48 us  [the longest x1 3.03 us: body(): got = lax.ppermute(away, 'tp', far)]
    all_to_all x2, starting transfers between devices: 12.9 us -> 11.3 us  [exchange(): lax.all_to_all(blocks, 'ep', split_axis=0, concat_axis=0, tiled=True)]
    all_to_all x2, waiting for transfers between devices: 19.2 us -> 18 us  [exchange(): lax.all_to_all(blocks, 'ep', split_axis=0, concat_axis=0, tiled=True)]
    another operation x1 -> x0, other arithmetic: 0.89 us -> none  [body(): jnp.stack([lax.dynamic_slice_in_dim(w, away, 2 * width, 1) for w in (gate...]
    convert_element_type x0 -> x1, other arithmetic: none -> 0.69 us  [body(): return (own + lax.ppermute(send, 'tp', near).astype(F32)).astype(BF16)]
  transfers between devices with their start and end apart: 7 -> 9, of which waited for: 5 -> 6; matrix products, arithmetic and copies ran while one was open for 2% -> 0% of each run, Pallas kernels for 1% -> 4%
where the time goes in v3:
time: 53 us; the launch traced here: 52.6 us
  waiting for transfers between devices  26.8 us (51%)
  starting transfers between devices  16.8 us (32%)
  local copies, waits for them, and re-layouts  4.34 us (8%)
  Pallas kernels  3.94 us (7%)
  other arithmetic  0.69 us (1%)
    all_to_all x2, waiting for transfers between devices, exchange(): lax.all_to_all(blocks, 'ep', split_axis=0, concat_axis=0, tiled=True)  18 us
    all_to_all x2, starting transfers between devices, exchange(): lax.all_to_all(blocks, 'ep', split_axis=0, concat_axis=0, tiled=True)  11.3 us
    ppermute x1, waiting for transfers between devices, body(): projected.append((full, lax.ppermute(send, 'tp', far)))  4.71 us
    unnamed x16, local copies, waits for them, and re-layouts  4.34 us
    pallas_call x6, Pallas kernels, call(): pl.pallas_call(kernel, out_shape=shapes, in_specs=[VM] * len(arrays) if s...  3.94 us
    ppermute x1, starting transfers between devices, body(): got = lax.ppermute(away, 'tp', far)  3.03 us
    ppermute x1, starting transfers between devices, body(): got_down = lax.ppermute(away_down, 'tp', far)  1.74 us
    ppermute x1, waiting for transfers between devices, body(): near_got_down = lax.ppermute(got_down, 'tp', near)  1.44 us
  transfers between devices with their start and end apart: 9, of which 6 were waited for; matrix products, arithmetic and copies ran while one was open for 0% of the time, Pallas kernels for 4%

profile of v3, /device:TPU:0, one launch (start us, length us, event | category | flops | bytes accessed | tf_op | source)
XLA Modules:
  0.0 52.6 jit_solution(16889754961934903761)
XLA Ops:
  0.0 1.0 %copy-done.1 = bf16[1,2048,96]{1,2,0:T(8,128)(2,1)S(1)} copy-done((bf16[1,2048,96]{1,2,0:T(8,128)(2,1)S(1)}, bf16[1,2048,96]{1,2,0:T(8,128)(2,1)}, u32[]{:S(2)}) %copy-start.1) | copy-done | bytes 393240
  1.0 1.0 %copy-done.2 = bf16[1,2048,96]{1,2,0:T(8,128)(2,1)S(1)} copy-done((bf16[1,2048,96]{1,2,0:T(8,128)(2,1)S(1)}, bf16[1,2048,96]{1,2,0:T(8,128)(2,1)}, u32[]{:S(2)}) %copy-start.2) | copy-done | bytes 393240
  2.0 1.0 %copy-done.3 = bf16[1,96,2048]{2,1,0:T(8,128)(2,1)S(1)} copy-done((bf16[1,96,2048]{2,1,0:T(8,128)(2,1)S(1)}, bf16[1,96,2048]{2,1,0:T(8,128)(2,1)}, u32[]{:S(2)}) %copy-start.3) | copy-done | bytes 393240
  3.0 0.2 shard_map.84
  3.2 3.0 %collective-permute-start = (bf16[2,96,1024]{2,1,0:T(8,128)(2,1)S(1)}, bf16[2,96,1024]{2,1,0:T(8,128)(2,1)S(1)}, u32[]{:S(2)}, u32[]{:S(2)}) collective-permute-start(bf16[2,96,1024]{2,1,0:T(8,128)(2,1)S(1)} %get-tuple-element.13), channel_id=1, source_target_pairs={{0,2},{1,3},{2,0},{3,1},{4,6},{5,7},{6,4},{7,5},{8,10},{9,11},{10,... | collective-permute-start | bytes 1179656 | tf_op jit(solution)/shard_map/ppermute | solution.py:192
  6.3 0.7 %copy-done.5 = s32[128,2]{0,1:T(2,128)S(1)} copy-done((s32[128,2]{0,1:T(2,128)S(1)}, s32[128,2]{0,1:T(2,128)}, u32[]{:S(2)}) %copy-start.5) | copy-done | bytes 1048
  6.9 1.2 %shard_map.83 = bf16[192,1024]{1,0:T(8,128)(2,1)} custom-call(bf16[128,2048]{1,0:T(8,128)(2,1)S(1)} %copy-done, f32[1,2048]{1,0:T(1,128)S(1)} %bitcast.20, s32[2,128]{1,0:T(2,128)S(1)} %bitcast.21), custom_call_target="tpu_custom_call" | custom-call | tf_op jit(solution)/shard_map/pallas_call | solution.py:152
  8.2 5.8 %all-to-all-start = ((bf16[8,24,1024]{2,1,0:T(8,128)(2,1)}), bf16[8,24,1024]{2,1,0:T(8,128)(2,1)S(1)}, u32[]{:S(2)}, u32[]{:S(2)}) async-start(bf16[8,24,1024]{2,1,0:T(8,128)(2,1)} %bitcast.4), calls=%async_computation | async-start | bytes 786432 | tf_op jit(solution)/shard_map/all_to_all | solution.py:181
  14.0 1.4 %collective-permute-done.far_ref = bf16[2,96,1024]{2,1,0:T(8,128)(2,1)S(1)} collective-permute-done((bf16[2,96,1024]{2,1,0:T(8,128)(2,1)S(1)}, bf16[2,96,1024]{2,1,0:T(8,128)(2,1)S(1)}, u32[]{:S(2)}, u32[]{:S(2)}) %collective-permute-start) | collective-permute-done | bytes 393248 | tf_op jit(solution)/shard_map/ppermute | solution.py:192
  15.4 1.7 %collective-permute-start.4 = (bf16[96,1024]{1,0:T(8,128)(2,1)S(1)}, bf16[96,1024]{1,0:T(8,128)(2,1)S(1)}, u32[]{:S(2)}, u32[]{:S(2)}) collective-permute-start(bf16[96,1024]{1,0:T(8,128)(2,1)S(1)} %get-tuple-element.16), channel_id=1, source_target_pairs={{0,2},{1,3},{2,0},{3,1},{4,6},{5,7},{6,4},{7,5},{8,10},{9,11},{10,... | collective-permute-start | bytes 589832 | tf_op jit(solution)/shard_map/ppermute | solution.py:193
  17.1 8.3 %all-to-all-done = bf16[8,24,1024]{2,1,0:T(8,128)(2,1)S(1)} async-done(((bf16[8,24,1024]{2,1,0:T(8,128)(2,1)}), bf16[8,24,1024]{2,1,0:T(8,128)(2,1)S(1)}, u32[]{:S(2)}, u32[]{:S(2)}) %all-to-all-start) | async-done | bytes 393248 | tf_op jit(solution)/shard_map/all_to_all | solution.py:181
  25.5 0.7 %shard_map.85 = (f32[192,768]{1,0:T(8,128)S(1)}, bf16[192,768]{1,0:T(8,128)(2,1)S(1)}) custom-call(bf16[192,1024]{1,0:T(8,128)(2,1)S(1)} %bitcast.15, bf16[3,96,1024]{2,1,0:T(8,128)(2,1)S(1)} %get-tuple-element.12.keep_ref, bf16[2,96,1024]{2,1,0:T(8,128)(2,1)S(1)} %collective-permute-done.far_ref, bf16[3,96,1024]{2,1,0:T(8,128)(2,1)S(1)} %collective-permute-done.1.near_ref, ...), custom_call_target="tpu_custom_call" | custom-call | tf_op jit(solution)/shard_map/pallas_call | solution.py:152
  26.2 0.6 %collective-permute-start.3 = (bf16[192,768]{1,0:T(8,128)(2,1)S(1)}, bf16[192,768]{1,0:T(8,128)(2,1)S(1)}, u32[]{:S(2)}, u32[]{:S(2)}) collective-permute-start(bf16[192,768]{1,0:T(8,128)(2,1)S(1)} %get-tuple-element.15), channel_id=1, source_target_pairs={{0,2},{1,3},{2,0},{3,1},{4,6},{5,7},{6,4},{7,5},{8,10},{9,11},{10,... | collective-permute-start | bytes 884744 | tf_op jit(solution)/shard_map/ppermute | solution.py:217
  26.8 1.4 %collective-permute-done.5.near_far_ref = bf16[96,1024]{1,0:T(8,128)(2,1)S(1)} collective-permute-done((bf16[96,1024]{1,0:T(8,128)(2,1)S(1)}, bf16[96,1024]{1,0:T(8,128)(2,1)S(1)}, u32[]{:S(2)}, u32[]{:S(2)}) %collective-permute-start.5) | collective-permute-done | bytes 196640 | tf_op jit(solution)/shard_map/ppermute | solution.py:196
  28.2 4.7 %collective-permute-done.3.got_ref = bf16[192,768]{1,0:T(8,128)(2,1)S(1)} collective-permute-done((bf16[192,768]{1,0:T(8,128)(2,1)S(1)}, bf16[192,768]{1,0:T(8,128)(2,1)S(1)}, u32[]{:S(2)}, u32[]{:S(2)}) %collective-permute-start.3) | collective-permute-done | bytes 294944 | tf_op jit(solution)/shard_map/ppermute | solution.py:217
  32.9 1.2 %shard_map.86 = bf16[192,1024]{1,0:T(8,128)(2,1)} custom-call(f32[192,768]{1,0:T(8,128)S(1)} %get-tuple-element.14.full_ref, bf16[192,768]{1,0:T(8,128)(2,1)S(1)} %collective-permute-done.3.got_ref, bf16[3,96,1024]{2,1,0:T(8,128)(2,1)S(1)} %get-tuple-element.12.keep_ref, bf16[96,1024]{1,0:T(8,128)(2,1)S(1)} %collective-permute-done.4.far_ref, ...), custom_call_target="tpu_custom_call" | custom-call | tf_op jit(solution)/shard_map/pallas_call | solution.py:152
  34.1 5.4 %all-to-all-start.1 = ((bf16[8,24,1024]{2,1,0:T(8,128)(2,1)}), bf16[8,24,1024]{2,1,0:T(8,128)(2,1)S(1)}, u32[]{:S(2)}, u32[]{:S(2)}) async-start(bf16[8,24,1024]{2,1,0:T(8,128)(2,1)} %bitcast.11), calls=%async_computation.1 | async-start | bytes 786432 | tf_op jit(solution)/shard_map/all_to_all | solution.py:181
  39.6 0.7 %copy-done.6 = f32[128,2]{0,1:T(2,128)S(1)} copy-done((f32[128,2]{0,1:T(2,128)S(1)}, f32[128,2]{0,1:T(2,128)}, u32[]{:S(2)}) %copy-start.6) | copy-done | bytes 1048
  40.2 0.3 shard_map.82.refs_0_
  40.6 9.6 %all-to-all-done.1 = bf16[8,24,1024]{2,1,0:T(8,128)(2,1)S(1)} async-done(((bf16[8,24,1024]{2,1,0:T(8,128)(2,1)}), bf16[8,24,1024]{2,1,0:T(8,128)(2,1)S(1)}, u32[]{:S(2)}, u32[]{:S(2)}) %all-to-all-start.1) | async-done | bytes 393248 | tf_op jit(solution)/shard_map/all_to_all | solution.py:181
  50.2 0.3 shard_map.87
  50.5 0.1 collective-permute-start.6
  50.6 1.3 %collective-permute-done.6 = bf16[128,512]{1,0:T(8,128)(2,1)S(1)} collective-permute-done((bf16[128,512]{1,0:T(8,128)(2,1)S(1)}, bf16[128,512]{1,0:T(8,128)(2,1)S(1)}, u32[]{:S(2)}, u32[]{:S(2)}) %collective-permute-start.6) | collective-permute-done | bytes 131104 | tf_op jit(solution)/shard_map/ppermute | solution.py:230
  51.9 0.7 %add_convert_fusion = bf16[128,512]{1,0:T(8,128)(2,1)} fusion(f32[128,512]{1,0:T(8,128)S(1)} %get-tuple-element.17, bf16[128,512]{1,0:T(8,128)(2,1)S(1)} %collective-permute-done.6), kind=kLoop, calls=%fused_computation | loop fusion | flops 196608 | bytes 524288 | tf_op jit(solution)/shard_map/convert_element_type | solution.py:230
  (17 shorter events, 0.0 us)
Async XLA Ops:
  0.0 1.0 %copy-start.1 = (bf16[1,2048,96]{1,2,0:T(8,128)(2,1)S(1)}, bf16[1,2048,96]{1,2,0:T(8,128)(2,1)}, u32[]{:S(2)}) copy-start(bf16[1,2048,96]{1,2,0:T(8,128)(2,1)} %param.13) | copy-start | bytes 1179652
  1.0 1.0 %copy-start.2 = (bf16[1,2048,96]{1,2,0:T(8,128)(2,1)S(1)}, bf16[1,2048,96]{1,2,0:T(8,128)(2,1)}, u32[]{:S(2)}) copy-start(bf16[1,2048,96]{1,2,0:T(8,128)(2,1)} %param.14) | copy-start | bytes 1179652
  2.0 1.0 %copy-start.3 = (bf16[1,96,2048]{2,1,0:T(8,128)(2,1)S(1)}, bf16[1,96,2048]{2,1,0:T(8,128)(2,1)}, u32[]{:S(2)}) copy-start(bf16[1,96,2048]{2,1,0:T(8,128)(2,1)} %param.15) | copy-start | bytes 1179652
  3.0 3.3 %copy-start = (bf16[128,2048]{1,0:T(8,128)(2,1)S(1)}, bf16[128,2048]{1,0:T(8,128)(2,1)}, u32[]{:S(2)}) copy-start(bf16[128,2048]{1,0:T(8,128)(2,1)} %tokens_ref.1) | copy-start | bytes 1572868
  3.0 3.3 %copy-start.4 = (f32[2048]{0:T(1024)S(1)}, f32[2048]{0:T(1024)}, u32[]{:S(2)}) copy-start(f32[2048]{0:T(1024)} %param.9) | copy-start | bytes 24580
  3.2 12.1 %collective-permute-start = (bf16[2,96,1024]{2,1,0:T(8,128)(2,1)S(1)}, bf16[2,96,1024]{2,1,0:T(8,128)(2,1)S(1)}, u32[]{:S(2)}, u32[]{:S(2)}) collective-permute-start(bf16[2,96,1024]{2,1,0:T(8,128)(2,1)S(1)} %get-tuple-element.13), channel_id=1, source_target_pairs={{0,2},{1,3},{2,0},{3,1},{4,6},{5,7},{6,4},{7,5},{8,10},{9,11},{10,... | collective-permute-start | bytes 1179656 | tf_op jit(solution)/shard_map/ppermute | solution.py:192
  6.3 0.7 %copy-start.5 = (s32[128,2]{0,1:T(2,128)S(1)}, s32[128,2]{0,1:T(2,128)}, u32[]{:S(2)}) copy-start(s32[128,2]{0,1:T(2,128)} %param.10) | copy-start | bytes 3076
  8.2 17.3 %all-to-all-start = ((bf16[8,24,1024]{2,1,0:T(8,128)(2,1)}), bf16[8,24,1024]{2,1,0:T(8,128)(2,1)S(1)}, u32[]{:S(2)}, u32[]{:S(2)}) async-start(bf16[8,24,1024]{2,1,0:T(8,128)(2,1)} %bitcast.4), calls=%async_computation | async-start | bytes 786432 | tf_op jit(solution)/shard_map/all_to_all | solution.py:181
  14.0 3.1 %collective-permute-start.1 = (bf16[3,96,1024]{2,1,0:T(8,128)(2,1)S(1)}, bf16[3,96,1024]{2,1,0:T(8,128)(2,1)S(1)}, u32[]{:S(2)}, u32[]{:S(2)}) collective-permute-start(bf16[3,96,1024]{2,1,0:T(8,128)(2,1)S(1)} %get-tuple-element.12.keep_ref), channel_id=1, source_target_pairs={{0,1},{1,0},{2,3},{3,2},{4,5},{5,4},{6,7},{7,6},{8,9},{9,8},{10,11... | collective-permute-start | bytes 1769480 | tf_op jit(solution)/shard_map/ppermute | solution.py:194
  15.4 10.1 %collective-permute-start.2 = (bf16[2,96,1024]{2,1,0:T(8,128)(2,1)S(1)}, bf16[2,96,1024]{2,1,0:T(8,128)(2,1)S(1)}, u32[]{:S(2)}, u32[]{:S(2)}) collective-permute-start(bf16[2,96,1024]{2,1,0:T(8,128)(2,1)S(1)} %collective-permute-done.far_ref), channel_id=1, source_target_pairs={{0,1},{1,0},{2,3},{3,2},{4,5},{5,4},{6,7},{7,6},{8,9},{9,8},{10,11... | collective-permute-start | bytes 1179656 | tf_op jit(solution)/shard_map/ppermute | solution.py:195
  15.4 11.4 %collective-permute-start.4 = (bf16[96,1024]{1,0:T(8,128)(2,1)S(1)}, bf16[96,1024]{1,0:T(8,128)(2,1)S(1)}, u32[]{:S(2)}, u32[]{:S(2)}) collective-permute-start(bf16[96,1024]{1,0:T(8,128)(2,1)S(1)} %get-tuple-element.16), channel_id=1, source_target_pairs={{0,2},{1,3},{2,0},{3,1},{4,6},{5,7},{6,4},{7,5},{8,10},{9,11},{10,... | collective-permute-start | bytes 589832 | tf_op jit(solution)/shard_map/ppermute | solution.py:193
  26.2 6.8 %collective-permute-start.3 = (bf16[192,768]{1,0:T(8,128)(2,1)S(1)}, bf16[192,768]{1,0:T(8,128)(2,1)S(1)}, u32[]{:S(2)}, u32[]{:S(2)}) collective-permute-start(bf16[192,768]{1,0:T(8,128)(2,1)S(1)} %get-tuple-element.15), channel_id=1, source_target_pairs={{0,2},{1,3},{2,0},{3,1},{4,6},{5,7},{6,4},{7,5},{8,10},{9,11},{10,... | collective-permute-start | bytes 884744 | tf_op jit(solution)/shard_map/ppermute | solution.py:217
  26.8 1.4 %collective-permute-start.5 = (bf16[96,1024]{1,0:T(8,128)(2,1)S(1)}, bf16[96,1024]{1,0:T(8,128)(2,1)S(1)}, u32[]{:S(2)}, u32[]{:S(2)}) collective-permute-start(bf16[96,1024]{1,0:T(8,128)(2,1)S(1)} %collective-permute-done.4.far_ref), channel_id=1, source_target_pairs={{0,1},{1,0},{2,3},{3,2},{4,5},{5,4},{6,7},{7,6},{8,9},{9,8},{10,11... | collective-permute-start | bytes 589832 | tf_op jit(solution)/shard_map/ppermute | solution.py:196
  34.1 16.1 %all-to-all-start.1 = ((bf16[8,24,1024]{2,1,0:T(8,128)(2,1)}), bf16[8,24,1024]{2,1,0:T(8,128)(2,1)S(1)}, u32[]{:S(2)}, u32[]{:S(2)}) async-start(bf16[8,24,1024]{2,1,0:T(8,128)(2,1)} %bitcast.11), calls=%async_computation.1 | async-start | bytes 786432 | tf_op jit(solution)/shard_map/all_to_all | solution.py:181
  39.6 0.7 %copy-start.6 = (f32[128,2]{0,1:T(2,128)S(1)}, f32[128,2]{0,1:T(2,128)}, u32[]{:S(2)}) copy-start(f32[128,2]{0,1:T(2,128)} %param.12) | copy-start | bytes 3076
  39.6 0.7 %copy-start.7 = (f32[128]{0:T(128)S(1)}, f32[128]{0:T(128)}, u32[]{:S(2)}) copy-start(f32[128]{0:T(128)} %param.11) | copy-start | bytes 1540
  50.5 1.4 %collective-permute-start.6 = (bf16[128,512]{1,0:T(8,128)(2,1)S(1)}, bf16[128,512]{1,0:T(8,128)(2,1)S(1)}, u32[]{:S(2)}, u32[]{:S(2)}) collective-permute-start(bf16[128,512]{1,0:T(8,128)(2,1)S(1)} %get-tuple-element.18), channel_id=1, source_target_pairs={{0,1},{1,0},{2,3},{3,2},{4,5},{5,4},{6,7},{7,6},{8,9},{9,8},{10,11... | collective-permute-start | bytes 393224 | tf_op jit(solution)/shard_map/ppermute | solution.py:230

commit v4 on v3

v4 whole, which is shorter than its diff:
```python
import functools

import jax
import jax.numpy as jnp
from jax import lax
from jax.experimental import pallas as pl
from jax.experimental.pallas import tpu as pltpu
from jax.sharding import PartitionSpec as P


F32, BF16, I32 = jnp.float32, jnp.bfloat16, jnp.int32
VM = pl.BlockSpec(memory_space=pltpu.VMEM)
HBM = pl.BlockSpec(memory_space=pltpu.HBM)


def dot(a, b, ca=1, cb=0):
    return lax.dot_general(a, b, (((ca,), (cb,)), ((), ())), preferred_element_type=F32)


def columns(index, width):
    return pl.ds(pl.multiple_of(index * width, width), width)


def iota(shape, axis):
    return lax.broadcasted_iota(I32, shape, axis)


def split(index, size):
    whole = ((index.astype(F32) + 0.5) * (1.0 / size)).astype(I32)
    return whole, index - size * whole


def mark(condition):
    return jnp.where(condition, 1.0, 0.0).astype(BF16)


def places(routes, experts):
    top, count = routes.shape
    expert_of = iota((experts, count), 0)
    named = routes[0:1] == expert_of
    for k in range(1, top):
        named = named | (routes[k : k + 1] == expert_of)
    ahead = iota((count, count), 0) < iota((count, count), 1)
    return jnp.where(named, dot(mark(named), mark(ahead)), -1.0).astype(BF16)


def pack_kernel(gate_hbm, up_hbm, tokens_hbm, gain_hbm, routes_hbm, *refs):
    away_ref, keep_ref, tokens_ref, gain_ref, routes_ref, sems = refs
    width = away_ref.shape[2]
    row = lax.axis_index("tp") >> 1
    here, there = columns(row, width), columns(1 - row, width)
    pairs = [
        (gate_hbm.at[:, there], away_ref.at[0]),
        (up_hbm.at[:, there], away_ref.at[1]),
        (tokens_hbm, tokens_ref),
        (gain_hbm, gain_ref),
        (routes_hbm, routes_ref),
        (gate_hbm.at[:, here], keep_ref.at[0]),
        (up_hbm.at[:, here], keep_ref.at[1]),
    ]
    copies = [pltpu.make_async_copy(a, b, sems.at[i]) for i, (a, b) in enumerate(pairs)]
    for copy in copies:
        copy.start()
    for copy in copies:
        copy.wait()


def dispatch_kernel(experts, half, tokens_ref, gain_ref, routes_ref, out_ref):
    width = out_ref.shape[1]
    q = lax.axis_index("tp")
    here = columns(q >> 1, width)
    values = tokens_ref[...].astype(F32)
    scale = lax.rsqrt(jnp.mean(values * values, -1, keepdims=True) + 1e-06)
    normed = (tokens_ref[:, here].astype(F32) * scale * gain_ref[:, here]).astype(BF16)
    rows = experts * half
    owner, _ = split(iota((rows, experts), 0), half)
    _, slot = split(iota((rows, 1), 0), half)
    place = places(routes_ref[...], experts)
    spread = mark(owner == iota((rows, experts), 1))
    held = dot(spread, place) == (slot + (q & 1) * half).astype(F32)
    out_ref[...] = dot(mark(held), normed).astype(BF16)


def gates_kernel(experts, quarter, ranks, routes_ref, prob_ref, logits_ref, out_ref):
    routes, logits = routes_ref[...], logits_ref[...]
    top, count = routes.shape
    powers = jnp.exp(logits - jnp.max(logits, 0, keepdims=True))
    weights = prob_ref[...] * (powers / jnp.sum(powers, 0, keepdims=True))
    expert_of = iota((experts, count), 0)
    by_expert = jnp.zeros((experts, count), F32)
    for k in range(top):
        by_expert = by_expert + jnp.where(routes[k : k + 1] == expert_of, weights[k : k + 1], 0.0)
    high = by_expert.astype(BF16)
    low = (by_expert - high.astype(F32)).astype(BF16)
    rows = experts * ranks * 2 * quarter
    owner, _ = split(iota((rows, experts), 0), ranks * 2 * quarter)
    _, inside = split(iota((rows, 1), 0), ranks * 2 * quarter)
    rank, inside = split(inside, 2 * quarter)
    _, slot = split(inside, quarter)
    slot = slot + ((rank & 1) * 2 + (rank >> 1)) * quarter
    spread = mark(owner == iota((rows, experts), 1))
    held = dot(spread, places(routes, experts)) == slot.astype(F32)
    for i, value in enumerate((high, low)):
        out_ref[i] = jnp.where(held, dot(spread, value), 0.0).T.astype(BF16)


def ordered(row, own, far):
    return [jnp.where(row == 0, own, far), jnp.where(row == 0, far, own)]


def project_kernel(quarter, mine_ref, keep_ref, far_ref, near_ref, near_far_ref, *out_refs):
    full_ref, send_ref = out_refs
    row = lax.axis_index("tp") >> 1
    rows = full_ref.shape[0]
    source, slot = split(iota((rows, 1), 0), quarter)
    at = source * 2 * quarter + slot
    slots = iota((rows, 2 * rows), 1)
    picks = jnp.concatenate(
        [mark(slots == at + row * quarter), mark(slots == at + (1 - row) * quarter)], 0
    )
    pieces = []
    for i in range(2):
        pieces += ordered(row, keep_ref[i], far_ref[i])
        pieces += ordered(row, near_ref[i], near_far_ref[i])
    picked = dot(picks, mine_ref[...]).astype(BF16)
    total = dot(picked, jnp.concatenate(pieces, 0), 1, 1)
    full_ref[...] = total[:rows]
    send_ref[...] = total[rows:].astype(BF16)


def expert_kernel(quarter, full_ref, got_ref, down_ref, far_ref, near_ref, near_far_ref, out_ref):
    row = lax.axis_index("tp") >> 1
    sources, ranks, _, width = out_ref.shape
    count = full_ref.shape[0]
    units = full_ref.shape[1] // 2
    gate = full_ref[:, :units] + got_ref[:, :units].astype(F32)
    up = full_ref[:, units:] + got_ref[:, units:].astype(F32)
    hidden = (gate / (1.0 + jnp.exp(-gate)) * up).astype(BF16)
    source, inside = split(iota((2 * count, 1), 0), 2 * quarter)
    part, slot = split(inside, quarter)
    twice = dot(mark(iota((2 * count, count), 1) == source * quarter + slot), hidden).astype(BF16)
    down = jnp.concatenate(
        ordered(row, down_ref[...], far_ref[...]) + ordered(row, near_ref[...], near_far_ref[...]),
        0,
    )
    for rank in range(ranks):
        first = 2 * rank * width
        both = dot(twice, down[:, first : first + 2 * width])
        chosen = jnp.where(part == 0, both[:, :width], both[:, width:])
        out_ref[:, rank] = chosen.reshape(sources, 2 * quarter, width).astype(BF16)


def combine_kernel(quarter, gates_ref, back_ref, out_ref):
    back = back_ref[...]
    width = back.shape[1]
    _, inside = split(iota((1, back.shape[0]), 1), 2 * quarter)
    for f in range(2):
        part = mark((inside >= quarter) == (f == 1))
        total = dot(gates_ref[0] * part, back) + dot(gates_ref[1] * part, back)
        out_ref[:, f * width : (f + 1) * width] = total.astype(BF16)


def call(kernel, shapes, arrays, specs=None, scratch=()):
    return pl.pallas_call(
        kernel,
        out_shape=shapes,
        in_specs=[VM] * len(arrays) if specs is None else specs,
        out_specs=jax.tree.map(lambda _: VM, shapes),
        scratch_shapes=scratch,
        compiler_params=pltpu.CompilerParams(vmem_limit_bytes=16 * 2**20),
    )(*arrays)


def body(tokens, norm_gain, routes, group_prob, expert_logits, gate_weight, up_weight, down_matrix):
    tok_rows, model_width = tokens.shape
    top = routes.shape[1]
    local, _, block = gate_weight.shape
    ep, tp = lax.axis_size("ep"), lax.axis_size("tp")
    experts = local * ep
    capacity = 3 * top * tok_rows // (2 * experts)
    quarter = -(-capacity // 4)
    half = 2 * quarter
    width = model_width // 2
    out_width = model_width // tp

    def shape(*dims, dtype=BF16):
        return jax.ShapeDtypeStruct(dims, dtype)

    near = [(i, i ^ 1) for i in range(tp)]
    far = [(i, i ^ 2) for i in range(tp)]

    down = down_matrix[0]
    held = [gate_weight[0].T, up_weight[0].T, tokens, norm_gain[None], routes.T]
    away, keep, *token_arrays = call(
        pack_kernel,
        (
            shape(2, block, width),
            shape(2, block, width),
            shape(*tokens.shape),
            shape(1, model_width, dtype=F32),
            shape(top, tok_rows, dtype=I32),
        ),
        [pltpu.with_memory_space_constraint(x, pltpu.HBM) for x in held],
        [HBM] * len(held),
        [pltpu.SemaphoreType.DMA((7,))],
    )
    got = lax.ppermute(away, "tp", far)
    got_down = lax.ppermute(down, "tp", far)
    near_keep = lax.ppermute(keep, "tp", near)
    near_down = lax.ppermute(down, "tp", near)
    near_got = lax.ppermute(got, "tp", near)
    near_got_down = lax.ppermute(got_down, "tp", near)

    outgoing = call(
        functools.partial(dispatch_kernel, experts, half),
        shape(experts * half, width),
        token_arrays,
    )
    gates = call(
        functools.partial(gates_kernel, experts, quarter, tp),
        shape(2, tok_rows, experts * tp * half),
        [token_arrays[2], group_prob[None], expert_logits.T],
    )
    mine = lax.all_to_all(
        outgoing.reshape(ep, half, width), "ep", split_axis=0, concat_axis=0, tiled=True
    ).reshape(ep * half, width)
    mine, gates = lax.optimization_barrier((mine, gates))
    full, send = call(
        functools.partial(project_kernel, quarter),
        (shape(ep * quarter, 2 * tp * block, dtype=F32), shape(ep * quarter, 2 * tp * block)),
        [mine, keep, got, near_keep, near_got],
    )
    partial = lax.ppermute(send, "tp", far)
    summed = call(
        functools.partial(expert_kernel, quarter),
        shape(ep, tp, half, out_width // 2),
        [full, partial, down, got_down, near_down, near_got_down],
    )
    back = lax.all_to_all(
        summed.reshape(ep * tp, half, out_width // 2),
        ("ep", "tp"),
        split_axis=0,
        concat_axis=0,
        tiled=True,
    ).reshape(ep * tp * half, out_width // 2)
    return call(
        functools.partial(combine_kernel, quarter), shape(tok_rows, out_width), [gates, back]
    )


def solution(mesh):
    return jax.shard_map(
        body,
        mesh=mesh,
        in_specs=(
            P("ep", None),
            P(),
            P("ep", None),
            P("ep"),
            P("ep", None),
            P("ep", None, "tp"),
            P("ep", None, "tp"),
            P("ep", "tp", None),
        ),
        out_specs=P("ep", "tp"),
        check_vma=False,
    )
```

time: 53 us -> 52.8 us (level)
  blocking collectives: 0 us -> 19.1 us
  waiting for transfers between devices: 26.8 us -> 13.8 us
  starting transfers between devices: 16.8 us -> 11.9 us
  local copies, waits for them, and re-layouts: 4.34 us -> 0.68 us
  Pallas kernels: 3.94 us -> 6.91 us
  other arithmetic: 0.69 us -> 0 us
    all_to_all x0 -> x1, blocking collectives: none -> 19.1 us  [body(): lax.all_to_all(summed.reshape(ep * tp, half, out_width // 2), ('ep', 'tp'...]
    all_to_all x2 -> x1, waiting for transfers between devices: 18 us -> 0.01 us  [body(): lax.all_to_all(outgoing.reshape(ep, half, width), 'ep', split_axis=0, con...]
    ppermute x3, waiting for transfers between devices: 6.05 us -> 12.1 us  [the longest x1 7.55 us: body(): got_down = lax.ppermute(down, 'tp', far)]
    all_to_all x2 -> x1, starting transfers between devices: 11.3 us -> 5.97 us  [body(): lax.all_to_all(outgoing.reshape(ep, half, width), 'ep', split_axis=0, con...]
    unnamed x16 -> x6, local copies, waits for them, and re-layouts: 4.34 us -> 0.68 us
    pallas_call x6, Pallas kernels: 3.94 us -> 6.91 us  [call(): pl.pallas_call(kernel, out_shape=shapes, in_specs=[VM] * len(arrays) if s...]
    ppermute x1, waiting for transfers between devices: 1.44 us -> 0.01 us  [body(): near_got_down = lax.ppermute(got_down, 'tp', near)]
    convert_element_type x1 -> x0, other arithmetic: 0.69 us -> none  [body(): return (own + lax.ppermute(send, 'tp', near).astype(F32)).astype(BF16)]
  transfers between devices with their start and end apart: 9 -> 8, of which waited for: 6 -> 3; matrix products, arithmetic and copies ran while one was open for 0% -> 0% of each run, Pallas kernels for 4% -> 7%
where the time goes in v4:
time: 52.8 us; the launch traced here: 52.5 us
  blocking collectives  19.1 us (36%)
  waiting for transfers between devices  13.8 us (26%)
  starting transfers between devices  11.9 us (23%)
  Pallas kernels  6.91 us (13%)
  local copies, waits for them, and re-layouts  0.68 us (1%)
    all_to_all x1, blocking collectives, body(): lax.all_to_all(summed.reshape(ep * tp, half, out_width // 2), ('ep', 'tp'...  19.1 us
    ppermute x1, waiting for transfers between devices, body(): got_down = lax.ppermute(down, 'tp', far)  7.55 us
    pallas_call x6, Pallas kernels, call(): pl.pallas_call(kernel, out_shape=shapes, in_specs=[VM] * len(arrays) if s...  6.91 us
    all_to_all x1, starting transfers between devices, body(): lax.all_to_all(outgoing.reshape(ep, half, width), 'ep', split_axis=0, con...  5.97 us
    ppermute x1, waiting for transfers between devices, body(): partial = lax.ppermute(send, 'tp', far)  4.54 us
    ppermute x1, starting transfers between devices, body(): got = lax.ppermute(away, 'tp', far)  3.03 us
    ppermute x1, starting transfers between devices, body(): partial = lax.ppermute(send, 'tp', far)  1.77 us
    ppermute x1, waiting for transfers between devices, body(): got = lax.ppermute(away, 'tp', far)  1.7 us
  transfers between devices with their start and end apart: 8, of which 3 were waited for; matrix products, arithmetic and copies ran while one was open for 0% of the time, Pallas kernels for 7%

profile of v4, /device:TPU:0, one launch (start us, length us, event | category | flops | bytes accessed | tf_op | source)
XLA Modules:
  0.0 52.5 jit_solution(5331147404418652093)
XLA Ops:
  0.0 1.4 %shard_map.82 = (bf16[2,96,1024]{2,1,0:T(8,128)(2,1)S(1)}, bf16[2,96,1024]{2,1,0:T(8,128)(2,1)S(1)}, bf16[128,2048]{1,0:T(8,128)(2,1)S(1)}, f32[1,2048]{1,0:T(1,128)S(1)}, s32[2,128]{1,0:T(2,128)S(1)}) custom-call(bf16[96,2048]{1,0:T(8,128)(2,1)} %bitcast.23, bf16[96,2048]{1,0:T(8,128)(2,1)} %bitcast.24, bf16[128,2048]{1,0:T(8,128)(2,1)} %tokens_hbm.1, ...), custom_call_target="tpu_custom_call" | custom-call | tf_op jit(solution)/shard_map/pallas_call | solution.py:164
  1.4 3.0 %collective-permute-start = (bf16[2,96,1024]{2,1,0:T(8,128)(2,1)S(1)}, bf16[2,96,1024]{2,1,0:T(8,128)(2,1)S(1)}, u32[]{:S(2)}, u32[]{:S(2)}) collective-permute-start(bf16[2,96,1024]{2,1,0:T(8,128)(2,1)S(1)} %get-tuple-element.20), channel_id=1, source_target_pairs={{0,2},{1,3},{2,0},{3,1},{4,6},{5,7},{6,4},{7,5},{8,10},{9,11},{10,... | collective-permute-start | bytes 1179656 | tf_op jit(solution)/shard_map/ppermute | solution.py:207
  4.5 1.2 %shard_map.83 = bf16[192,1024]{1,0:T(8,128)(2,1)} custom-call(bf16[128,2048]{1,0:T(8,128)(2,1)S(1)} %get-tuple-element.14.tokens_ref, f32[1,2048]{1,0:T(1,128)S(1)} %get-tuple-element.15.gain_ref, s32[2,128]{1,0:T(2,128)S(1)} %get-tuple-element.16.routes_ref), custom_call_target="tpu_custom_call" | custom-call | tf_op jit(solution)/shard_map/pallas_call | solution.py:164
  5.7 6.0 %all-to-all-start = ((bf16[8,24,1024]{2,1,0:T(8,128)(2,1)}), bf16[8,24,1024]{2,1,0:T(8,128)(2,1)S(1)}, u32[]{:S(2)}, u32[]{:S(2)}) async-start(bf16[8,24,1024]{2,1,0:T(8,128)(2,1)} %bitcast.6), calls=%async_computation | async-start | bytes 786432 | tf_op jit(solution)/shard_map/all_to_all | solution.py:224
  11.7 0.6 %collective-permute-start.4 = (bf16[96,2048]{1,0:T(8,128)(2,1)S(1)}, bf16[96,2048]{1,0:T(8,128)(2,1)S(1)}, u32[]{:S(2)}, u32[]{:S(2)}) collective-permute-start(bf16[96,2048]{1,0:T(8,128)(2,1)S(1)} %bitcast.18), channel_id=1, source_target_pairs={{0,2},{1,3},{2,0},{3,1},{4,6},{5,7},{6,4},{7,5},{8,10},{9,11},{10,... | collective-permute-start | bytes 1179656 | tf_op jit(solution)/shard_map/ppermute | solution.py:208
  12.3 0.0 collective-permute-start.1
  12.3 1.7 %collective-permute-done.far_ref = bf16[2,96,1024]{2,1,0:T(8,128)(2,1)S(1)} collective-permute-done((bf16[2,96,1024]{2,1,0:T(8,128)(2,1)S(1)}, bf16[2,96,1024]{2,1,0:T(8,128)(2,1)S(1)}, u32[]{:S(2)}, u32[]{:S(2)}) %collective-permute-start) | collective-permute-done | bytes 393248 | tf_op jit(solution)/shard_map/ppermute | solution.py:207
  14.0 0.0 collective-permute-start.2
  14.0 0.5 collective-permute-start.5
  14.5 7.5 %collective-permute-done.4.far_ref = bf16[96,2048]{1,0:T(8,128)(2,1)S(1)} collective-permute-done((bf16[96,2048]{1,0:T(8,128)(2,1)S(1)}, bf16[96,2048]{1,0:T(8,128)(2,1)S(1)}, u32[]{:S(2)}, u32[]{:S(2)}) %collective-permute-start.4) | collective-permute-done | bytes 393248 | tf_op jit(solution)/shard_map/ppermute | solution.py:208
  22.0 0.0 collective-permute-start.6
  22.0 0.7 %copy-done.1 = f32[128,2]{0,1:T(2,128)S(1)} copy-done((f32[128,2]{0,1:T(2,128)S(1)}, f32[128,2]{0,1:T(2,128)}, u32[]{:S(2)}) %copy-start.1) | copy-done | bytes 1048
  22.7 0.8 %shard_map.84.gates_ref = bf16[2,128,768]{2,1,0:T(8,128)(2,1)S(1)} custom-call(s32[2,128]{1,0:T(2,128)S(1)} %get-tuple-element.16.routes_ref, f32[1,128]{1,0:T(1,128)S(1)} %bitcast.22, f32[2,128]{1,0:T(2,128)S(1)} %bitcast.21), custom_call_target="tpu_custom_call" | custom-call | tf_op jit(solution)/shard_map/pallas_call | solution.py:164
  23.5 0.0 all-to-all-done
  23.5 0.0 collective-permute-done.1.near_ref
  23.5 0.0 collective-permute-done.2.near_far_ref
  23.5 1.7 %shard_map.85 = (f32[96,768]{1,0:T(8,128)S(1)}, bf16[96,768]{1,0:T(8,128)(2,1)S(1)}) custom-call(bf16[192,1024]{1,0:T(8,128)(2,1)S(1)} %bitcast.17, bf16[2,96,1024]{2,1,0:T(8,128)(2,1)S(1)} %get-tuple-element.19.keep_ref, bf16[2,96,1024]{2,1,0:T(8,128)(2,1)S(1)} %collective-permute-done.far_ref, bf16[2,96,1024]{2,1,0:T(8,128)(2,1)S(1)} %collective-permute-done.1.near_ref, ...), custom_call_target="tpu_custom_call" | custom-call | tf_op jit(solution)/shard_map/pallas_call | solution.py:164
  25.3 1.8 %collective-permute-start.3 = (bf16[96,768]{1,0:T(8,128)(2,1)S(1)}, bf16[96,768]{1,0:T(8,128)(2,1)S(1)}, u32[]{:S(2)}, u32[]{:S(2)}) collective-permute-start(bf16[96,768]{1,0:T(8,128)(2,1)S(1)} %get-tuple-element.22), channel_id=1, source_target_pairs={{0,2},{1,3},{2,0},{3,1},{4,6},{5,7},{6,4},{7,5},{8,10},{9,11},{10,... | collective-permute-start | bytes 442376 | tf_op jit(solution)/shard_map/ppermute | solution.py:233
  27.0 0.0 collective-permute-done.5.near_ref
  27.0 0.0 collective-permute-done.6.near_far_ref
  27.0 4.5 %collective-permute-done.3.got_ref = bf16[96,768]{1,0:T(8,128)(2,1)S(1)} collective-permute-done((bf16[96,768]{1,0:T(8,128)(2,1)S(1)}, bf16[96,768]{1,0:T(8,128)(2,1)S(1)}, u32[]{:S(2)}, u32[]{:S(2)}) %collective-permute-start.3) | collective-permute-done | bytes 147488 | tf_op jit(solution)/shard_map/ppermute | solution.py:233
  31.6 0.7 %shard_map.86 = bf16[8,4,24,256]{3,2,1,0:T(8,128)(2,1)S(1)} custom-call(f32[96,768]{1,0:T(8,128)S(1)} %get-tuple-element.21.full_ref, bf16[96,768]{1,0:T(8,128)(2,1)S(1)} %collective-permute-done.3.got_ref, bf16[96,2048]{1,0:T(8,128)(2,1)S(1)} %bitcast.20, bf16[96,2048]{1,0:T(8,128)(2,1)S(1)} %collective-permute-done.4.far_ref, ...), custom_call_target="tpu_custom_call" | custom-call | tf_op jit(solution)/shard_map/pallas_call | solution.py:164
  32.3 19.1 %all_to_all.10 = bf16[32,24,256]{2,1,0:T(8,128)(2,1)S(1)} all-to-all(bf16[32,24,256]{2,1,0:T(8,128)(2,1)S(1)} %bitcast.15), channel_id=1, replica_groups=mesh['ep'=8,'tp'=4] {'ep','tp'}, dimensions={0} | all-to-all | bytes 786432 | tf_op jit(solution)/shard_map/all_to_all | solution.py:239
  51.4 1.0 %shard_map.87 = bf16[128,512]{1,0:T(8,128)(2,1)} custom-call(bf16[2,128,768]{2,1,0:T(8,128)(2,1)S(1)} %shard_map.84.gates_ref, bf16[768,256]{1,0:T(8,128)(2,1)S(1)} %bitcast.16), custom_call_target="tpu_custom_call" | custom-call | tf_op jit(solution)/shard_map/pallas_call | solution.py:164
  (5 shorter events, 0.0 us)
Async XLA Ops:
  1.4 12.5 %collective-permute-start = (bf16[2,96,1024]{2,1,0:T(8,128)(2,1)S(1)}, bf16[2,96,1024]{2,1,0:T(8,128)(2,1)S(1)}, u32[]{:S(2)}, u32[]{:S(2)}) collective-permute-start(bf16[2,96,1024]{2,1,0:T(8,128)(2,1)S(1)} %get-tuple-element.20), channel_id=1, source_target_pairs={{0,2},{1,3},{2,0},{3,1},{4,6},{5,7},{6,4},{7,5},{8,10},{9,11},{10,... | collective-permute-start | bytes 1179656 | tf_op jit(solution)/shard_map/ppermute | solution.py:207
  5.7 6.0 %copy-start = (bf16[1,96,2048]{2,1,0:T(8,128)(2,1)S(1)}, bf16[1,96,2048]{2,1,0:T(8,128)(2,1)}, u32[]{:S(2)}) copy-start(bf16[1,96,2048]{2,1,0:T(8,128)(2,1)} %param.15) | copy-start | bytes 1179652
  5.7 17.8 %all-to-all-start = ((bf16[8,24,1024]{2,1,0:T(8,128)(2,1)}), bf16[8,24,1024]{2,1,0:T(8,128)(2,1)S(1)}, u32[]{:S(2)}, u32[]{:S(2)}) async-start(bf16[8,24,1024]{2,1,0:T(8,128)(2,1)} %bitcast.6), calls=%async_computation | async-start | bytes 786432 | tf_op jit(solution)/shard_map/all_to_all | solution.py:224
  11.7 10.4 %collective-permute-start.4 = (bf16[96,2048]{1,0:T(8,128)(2,1)S(1)}, bf16[96,2048]{1,0:T(8,128)(2,1)S(1)}, u32[]{:S(2)}, u32[]{:S(2)}) collective-permute-start(bf16[96,2048]{1,0:T(8,128)(2,1)S(1)} %bitcast.18), channel_id=1, source_target_pairs={{0,2},{1,3},{2,0},{3,1},{4,6},{5,7},{6,4},{7,5},{8,10},{9,11},{10,... | collective-permute-start | bytes 1179656 | tf_op jit(solution)/shard_map/ppermute | solution.py:208
  12.3 11.2 %collective-permute-start.1 = (bf16[2,96,1024]{2,1,0:T(8,128)(2,1)S(1)}, bf16[2,96,1024]{2,1,0:T(8,128)(2,1)S(1)}, u32[]{:S(2)}, u32[]{:S(2)}) collective-permute-start(bf16[2,96,1024]{2,1,0:T(8,128)(2,1)S(1)} %get-tuple-element.19.keep_ref), channel_id=1, source_target_pairs={{0,1},{1,0},{2,3},{3,2},{4,5},{5,4},{6,7},{7,6},{8,9},{9,8},{10,11... | collective-permute-start | bytes 1179656 | tf_op jit(solution)/shard_map/ppermute | solution.py:209
  14.0 9.5 %collective-permute-start.2 = (bf16[2,96,1024]{2,1,0:T(8,128)(2,1)S(1)}, bf16[2,96,1024]{2,1,0:T(8,128)(2,1)}, u32[]{:S(2)}, u32[]{:S(2)}) collective-permute-start(bf16[2,96,1024]{2,1,0:T(8,128)(2,1)S(1)} %collective-permute-done.far_ref), channel_id=1, source_target_pairs={{0,1},{1,0},{2,3},{3,2},{4,5},{5,4},{6,7},{7,6},{8,9},{9,8},{10,11... | collective-permute-start | bytes 1179656 | tf_op jit(solution)/shard_map/ppermute | solution.py:211
  14.0 13.0 %collective-permute-start.5 = (bf16[96,2048]{1,0:T(8,128)(2,1)S(1)}, bf16[96,2048]{1,0:T(8,128)(2,1)S(1)}, u32[]{:S(2)}, u32[]{:S(2)}) collective-permute-start(bf16[96,2048]{1,0:T(8,128)(2,1)S(1)} %bitcast.19), channel_id=1, source_target_pairs={{0,1},{1,0},{2,3},{3,2},{4,5},{5,4},{6,7},{7,6},{8,9},{9,8},{10,11... | collective-permute-start | bytes 1179656 | tf_op jit(solution)/shard_map/ppermute | solution.py:210
  22.0 5.0 %collective-permute-start.6 = (bf16[96,2048]{1,0:T(8,128)(2,1)S(1)}, bf16[96,2048]{1,0:T(8,128)(2,1)S(1)}, u32[]{:S(2)}, u32[]{:S(2)}) collective-permute-start(bf16[96,2048]{1,0:T(8,128)(2,1)S(1)} %collective-permute-done.4.far_ref), channel_id=1, source_target_pairs={{0,1},{1,0},{2,3},{3,2},{4,5},{5,4},{6,7},{7,6},{8,9},{9,8},{10,11... | collective-permute-start | bytes 1179656 | tf_op jit(solution)/shard_map/ppermute | solution.py:212
  22.0 0.7 %copy-start.1 = (f32[128,2]{0,1:T(2,128)S(1)}, f32[128,2]{0,1:T(2,128)}, u32[]{:S(2)}) copy-start(f32[128,2]{0,1:T(2,128)} %param.12) | copy-start | bytes 3076
  22.0 0.7 %copy-start.2 = (f32[128]{0:T(128)S(1)}, f32[128]{0:T(128)}, u32[]{:S(2)}) copy-start(f32[128]{0:T(128)} %param.11) | copy-start | bytes 1540
  25.3 6.3 %collective-permute-start.3 = (bf16[96,768]{1,0:T(8,128)(2,1)S(1)}, bf16[96,768]{1,0:T(8,128)(2,1)S(1)}, u32[]{:S(2)}, u32[]{:S(2)}) collective-permute-start(bf16[96,768]{1,0:T(8,128)(2,1)S(1)} %get-tuple-element.22), channel_id=1, source_target_pairs={{0,2},{1,3},{2,0},{3,1},{4,6},{5,7},{6,4},{7,5},{8,10},{9,11},{10,... | collective-permute-start | bytes 442376 | tf_op jit(solution)/shard_map/ppermute | solution.py:233

commit v5 on v4

--- a/solution.py
+++ b/solution.py
@@ -44,41 +44,41 @@
     return jnp.where(named, dot(mark(named), mark(ahead)), -1.0).astype(BF16)
 
 
-def pack_kernel(gate_hbm, up_hbm, tokens_hbm, gain_hbm, routes_hbm, *refs):
-    away_ref, keep_ref, tokens_ref, gain_ref, routes_ref, sems = refs
-    width = away_ref.shape[2]
-    row = lax.axis_index("tp") >> 1
+def front_kernel(
+    experts, half, tokens_hbm, gain_hbm, routes_hbm, gate_hbm, up_hbm, *refs
+):
+    out_ref, away_ref, keep_ref, tokens_ref, gain_ref, routes_ref, sems = refs
+    width = out_ref.shape[1]
+    q = lax.axis_index("tp")
+    row = q >> 1
     here, there = columns(row, width), columns(1 - row, width)
     pairs = [
-        (gate_hbm.at[:, there], away_ref.at[0]),
-        (up_hbm.at[:, there], away_ref.at[1]),
         (tokens_hbm, tokens_ref),
         (gain_hbm, gain_ref),
         (routes_hbm, routes_ref),
+        (gate_hbm.at[:, there], away_ref.at[0]),
+        (up_hbm.at[:, there], away_ref.at[1]),
         (gate_hbm.at[:, here], keep_ref.at[0]),
         (up_hbm.at[:, here], keep_ref.at[1]),
     ]
     copies = [pltpu.make_async_copy(a, b, sems.at[i]) for i, (a, b) in enumerate(pairs)]
     for copy in copies:
         copy.start()
-    for copy in copies:
-        copy.wait()
-
-
-def dispatch_kernel(experts, half, tokens_ref, gain_ref, routes_ref, out_ref):
-    width = out_ref.shape[1]
-    q = lax.axis_index("tp")
-    here = columns(q >> 1, width)
+    rows = experts * half
+    owner, _ = split(iota((rows, experts), 0), half)
+    _, slot = split(iota((rows, 1), 0), half)
+    copies[2].wait()
+    place = places(routes_ref[...], experts)
+    spread = mark(owner == iota((rows, experts), 1))
+    held = mark(dot(spread, place) == (slot + (q & 1) * half).astype(F32))
+    copies[0].wait()
+    copies[1].wait()
     values = tokens_ref[...].astype(F32)
     scale = lax.rsqrt(jnp.mean(values * values, -1, keepdims=True) + 1e-06)
     normed = (tokens_ref[:, here].astype(F32) * scale * gain_ref[:, here]).astype(BF16)
-    rows = experts * half
-    owner, _ = split(iota((rows, experts), 0), half)
-    _, slot = split(iota((rows, 1), 0), half)
-    place = places(routes_ref[...], experts)
-    spread = mark(owner == iota((rows, experts), 1))
-    held = dot(spread, place) == (slot + (q & 1) * half).astype(F32)
-    out_ref[...] = dot(mark(held), normed).astype(BF16)
+    out_ref[...] = dot(held, normed).astype(BF16)
+    for copy in copies[3:]:
+        copy.wait()
 
 
 def gates_kernel(experts, quarter, ranks, routes_ref, prob_ref, logits_ref, out_ref):
@@ -190,19 +190,18 @@
     far = [(i, i ^ 2) for i in range(tp)]
 
     down = down_matrix[0]
-    held = [gate_weight[0].T, up_weight[0].T, tokens, norm_gain[None], routes.T]
-    away, keep, *token_arrays = call(
-        pack_kernel,
-        (
-            shape(2, block, width),
-            shape(2, block, width),
-            shape(*tokens.shape),
-            shape(1, model_width, dtype=F32),
-            shape(top, tok_rows, dtype=I32),
-        ),
-        [pltpu.with_memory_space_constraint(x, pltpu.HBM) for x in held],
-        [HBM] * len(held),
-        [pltpu.SemaphoreType.DMA((7,))],
+    inputs = [tokens, norm_gain[None], routes.T, gate_weight[0].T, up_weight[0].T]
+    outgoing, away, keep = call(
+        functools.partial(front_kernel, experts, half),
+        (shape(experts * half, width), shape(2, block, width), shape(2, block, width)),
+        [pltpu.with_memory_space_constraint(x, pltpu.HBM) for x in inputs],
+        [HBM] * len(inputs),
+        [
+            pltpu.VMEM(tokens.shape, BF16),
+            pltpu.VMEM((1, model_width), F32),
+            pltpu.VMEM((top, tok_rows), I32),
+            pltpu.SemaphoreType.DMA((7,)),
+        ],
     )
     got = lax.ppermute(away, "tp", far)
     got_down = lax.ppermute(down, "tp", far)
@@ -211,15 +210,10 @@
     near_got = lax.ppermute(got, "tp", near)
     near_got_down = lax.ppermute(got_down, "tp", near)
 
-    outgoing = call(
-        functools.partial(dispatch_kernel, experts, half),
-        shape(experts * half, width),
-        token_arrays,
-    )
     gates = call(
         functools.partial(gates_kernel, experts, quarter, tp),
         shape(2, tok_rows, experts * tp * half),
-        [token_arrays[2], group_prob[None], expert_logits.T],
+        [routes.T, group_prob[None], expert_logits.T],
     )
     mine = lax.all_to_all(
         outgoing.reshape(ep, half, width), "ep", split_axis=0, concat_axis=0, tiled=True

time: 52.8 us -> 53.7 us (1.017)
  waiting for transfers between devices: 13.8 us -> 15 us
    ppermute x1, waiting for transfers between devices: 1.7 us -> 3.39 us  [body(): got = lax.ppermute(away, 'tp', far)]
    pallas_call x6 -> x5, Pallas kernels: 6.91 us -> 6.62 us  [call(): pl.pallas_call(kernel, out_shape=shapes, in_specs=[VM] * len(arrays) if s...]
  transfers between devices with their start and end apart: 8 -> 8, of which waited for: 3 -> 3; matrix products, arithmetic and copies ran while one was open for 0% -> 0% of each run, Pallas kernels for 7% -> 5%
where the time goes in v5:
time: 53.7 us; the launch traced here: 53.4 us
  blocking collectives  19.1 us (36%)
  waiting for transfers between devices  15 us (28%)
  starting transfers between devices  11.9 us (22%)
  Pallas kernels  6.62 us (12%)
  local copies, waits for them, and re-layouts  0.68 us (1%)
    all_to_all x1, blocking collectives, body(): lax.all_to_all(summed.reshape(ep * tp, half, out_width // 2), ('ep', 'tp'...  19.1 us
    ppermute x1, waiting for transfers between devices, body(): got_down = lax.ppermute(down, 'tp', far)  7.05 us
    pallas_call x5, Pallas kernels, call(): pl.pallas_call(kernel, out_shape=shapes, in_specs=[VM] * len(arrays) if s...  6.62 us
    all_to_all x1, starting transfers between devices, body(): lax.all_to_all(outgoing.reshape(ep, half, width), 'ep', split_axis=0, con...  5.96 us
    ppermute x1, waiting for transfers between devices, body(): partial = lax.ppermute(send, 'tp', far)  4.51 us
    ppermute x1, waiting for transfers between devices, body(): got = lax.ppermute(away, 'tp', far)  3.39 us
    ppermute x1, starting transfers between devices, body(): got = lax.ppermute(away, 'tp', far)  3.04 us
    ppermute x1, starting transfers between devices, body(): partial = lax.ppermute(send, 'tp', far)  1.81 us
  transfers between devices with their start and end apart: 8, of which 3 were waited for; matrix products, arithmetic and copies ran while one was open for 0% of the time, Pallas kernels for 5%

profile of v5, /device:TPU:0, one launch (start us, length us, event | category | flops | bytes accessed | tf_op | source)
XLA Modules:
  0.0 53.4 jit_solution(11215240729732515080)
XLA Ops:
  0.0 2.4 %shard_map.82 = (bf16[192,1024]{1,0:T(8,128)(2,1)}, bf16[2,96,1024]{2,1,0:T(8,128)(2,1)S(1)}, bf16[2,96,1024]{2,1,0:T(8,128)(2,1)S(1)}) custom-call(bf16[128,2048]{1,0:T(8,128)(2,1)} %tokens_hbm.1, f32[1,2048]{1,0:T(1,128)} %bitcast.27, s32[2,128]{1,0:T(2,128)} %bitcast.21, bf16[96,2048]{1,0:T(8,128)(2,1)} %bitcast.25, bf16[96,2048]{1,0:T(8,128)(2,1)} %bitcast.26), custom_call_target="tpu_custom_call" | custom-call | tf_op jit(solution)/shard_map/pallas_call | solution.py:164
  2.4 3.0 %collective-permute-start = (bf16[2,96,1024]{2,1,0:T(8,128)(2,1)S(1)}, bf16[2,96,1024]{2,1,0:T(8,128)(2,1)S(1)}, u32[]{:S(2)}, u32[]{:S(2)}) collective-permute-start(bf16[2,96,1024]{2,1,0:T(8,128)(2,1)S(1)} %get-tuple-element.16), channel_id=1, source_target_pairs={{0,2},{1,3},{2,0},{3,1},{4,6},{5,7},{6,4},{7,5},{8,10},{9,11},{10,... | collective-permute-start | bytes 1179656 | tf_op jit(solution)/shard_map/ppermute | solution.py:206
  5.4 6.0 %all-to-all-start = ((bf16[8,24,1024]{2,1,0:T(8,128)(2,1)}), bf16[8,24,1024]{2,1,0:T(8,128)(2,1)S(1)}, u32[]{:S(2)}, u32[]{:S(2)}) async-start(bf16[8,24,1024]{2,1,0:T(8,128)(2,1)} %bitcast.6), calls=%async_computation | async-start | bytes 786432 | tf_op jit(solution)/shard_map/all_to_all | solution.py:218
  11.4 0.6 %collective-permute-start.4 = (bf16[96,2048]{1,0:T(8,128)(2,1)S(1)}, bf16[96,2048]{1,0:T(8,128)(2,1)S(1)}, u32[]{:S(2)}, u32[]{:S(2)}) collective-permute-start(bf16[96,2048]{1,0:T(8,128)(2,1)S(1)} %bitcast.18), channel_id=1, source_target_pairs={{0,2},{1,3},{2,0},{3,1},{4,6},{5,7},{6,4},{7,5},{8,10},{9,11},{10,... | collective-permute-start | bytes 1179656 | tf_op jit(solution)/shard_map/ppermute | solution.py:207
  12.0 0.0 collective-permute-start.1
  12.0 3.4 %collective-permute-done.far_ref = bf16[2,96,1024]{2,1,0:T(8,128)(2,1)S(1)} collective-permute-done((bf16[2,96,1024]{2,1,0:T(8,128)(2,1)S(1)}, bf16[2,96,1024]{2,1,0:T(8,128)(2,1)S(1)}, u32[]{:S(2)}, u32[]{:S(2)}) %collective-permute-start) | collective-permute-done | bytes 393248 | tf_op jit(solution)/shard_map/ppermute | solution.py:206
  15.4 0.0 collective-permute-start.2
  15.4 0.5 collective-permute-start.5
  15.9 7.1 %collective-permute-done.4.far_ref = bf16[96,2048]{1,0:T(8,128)(2,1)S(1)} collective-permute-done((bf16[96,2048]{1,0:T(8,128)(2,1)S(1)}, bf16[96,2048]{1,0:T(8,128)(2,1)S(1)}, u32[]{:S(2)}, u32[]{:S(2)}) %collective-permute-start.4) | collective-permute-done | bytes 393248 | tf_op jit(solution)/shard_map/ppermute | solution.py:207
  22.9 0.0 collective-permute-start.6
  23.0 0.7 %copy-done.1 = s32[128,2]{0,1:T(2,128)S(1)} copy-done((s32[128,2]{0,1:T(2,128)S(1)}, s32[128,2]{0,1:T(2,128)}, u32[]{:S(2)}) %copy-start.1) | copy-done | bytes 1048
  23.6 0.0 copy-done.3
  23.6 0.8 %shard_map.83.gates_ref = bf16[2,128,768]{2,1,0:T(8,128)(2,1)S(1)} custom-call(s32[2,128]{1,0:T(2,128)S(1)} %bitcast.22, f32[1,128]{1,0:T(1,128)S(1)} %bitcast.24, f32[2,128]{1,0:T(2,128)S(1)} %bitcast.23), custom_call_target="tpu_custom_call" | custom-call | tf_op jit(solution)/shard_map/pallas_call | solution.py:164
  24.4 0.0 all-to-all-done
  24.4 0.0 collective-permute-done.1.near_ref
  24.4 0.0 collective-permute-done.2.near_far_ref
  24.4 1.7 %shard_map.84 = (f32[96,768]{1,0:T(8,128)S(1)}, bf16[96,768]{1,0:T(8,128)(2,1)S(1)}) custom-call(bf16[192,1024]{1,0:T(8,128)(2,1)S(1)} %bitcast.17, bf16[2,96,1024]{2,1,0:T(8,128)(2,1)S(1)} %get-tuple-element.15.keep_ref, bf16[2,96,1024]{2,1,0:T(8,128)(2,1)S(1)} %collective-permute-done.far_ref, bf16[2,96,1024]{2,1,0:T(8,128)(2,1)S(1)} %collective-permute-done.1.near_ref, ...), custom_call_target="tpu_custom_call" | custom-call | tf_op jit(solution)/shard_map/pallas_call | solution.py:164
  26.2 1.8 %collective-permute-start.3 = (bf16[96,768]{1,0:T(8,128)(2,1)S(1)}, bf16[96,768]{1,0:T(8,128)(2,1)S(1)}, u32[]{:S(2)}, u32[]{:S(2)}) collective-permute-start(bf16[96,768]{1,0:T(8,128)(2,1)S(1)} %get-tuple-element.18), channel_id=1, source_target_pairs={{0,2},{1,3},{2,0},{3,1},{4,6},{5,7},{6,4},{7,5},{8,10},{9,11},{10,... | collective-permute-start | bytes 442376 | tf_op jit(solution)/shard_map/ppermute | solution.py:227
  28.0 0.0 collective-permute-done.5.near_ref
  28.0 0.0 collective-permute-done.6.near_far_ref
  28.0 4.5 %collective-permute-done.3.got_ref = bf16[96,768]{1,0:T(8,128)(2,1)S(1)} collective-permute-done((bf16[96,768]{1,0:T(8,128)(2,1)S(1)}, bf16[96,768]{1,0:T(8,128)(2,1)S(1)}, u32[]{:S(2)}, u32[]{:S(2)}) %collective-permute-start.3) | collective-permute-done | bytes 147488 | tf_op jit(solution)/shard_map/ppermute | solution.py:227
  32.5 0.7 %shard_map.85 = bf16[8,4,24,256]{3,2,1,0:T(8,128)(2,1)S(1)} custom-call(f32[96,768]{1,0:T(8,128)S(1)} %get-tuple-element.17.full_ref, bf16[96,768]{1,0:T(8,128)(2,1)S(1)} %collective-permute-done.3.got_ref, bf16[96,2048]{1,0:T(8,128)(2,1)S(1)} %bitcast.20, bf16[96,2048]{1,0:T(8,128)(2,1)S(1)} %collective-permute-done.4.far_ref, ...), custom_call_target="tpu_custom_call" | custom-call | tf_op jit(solution)/shard_map/pallas_call | solution.py:164
  33.2 19.1 %all_to_all.10 = bf16[32,24,256]{2,1,0:T(8,128)(2,1)S(1)} all-to-all(bf16[32,24,256]{2,1,0:T(8,128)(2,1)S(1)} %bitcast.15), channel_id=1, replica_groups=mesh['ep'=8,'tp'=4] {'ep','tp'}, dimensions={0} | all-to-all | bytes 786432 | tf_op jit(solution)/shard_map/all_to_all | solution.py:233
  52.4 1.0 %shard_map.86 = bf16[128,512]{1,0:T(8,128)(2,1)} custom-call(bf16[2,128,768]{2,1,0:T(8,128)(2,1)S(1)} %shard_map.83.gates_ref, bf16[768,256]{1,0:T(8,128)(2,1)S(1)} %bitcast.16), custom_call_target="tpu_custom_call" | custom-call | tf_op jit(solution)/shard_map/pallas_call | solution.py:164
  (6 shorter events, 0.0 us)
Async XLA Ops:
  2.4 13.0 %collective-permute-start = (bf16[2,96,1024]{2,1,0:T(8,128)(2,1)S(1)}, bf16[2,96,1024]{2,1,0:T(8,128)(2,1)S(1)}, u32[]{:S(2)}, u32[]{:S(2)}) collective-permute-start(bf16[2,96,1024]{2,1,0:T(8,128)(2,1)S(1)} %get-tuple-element.16), channel_id=1, source_target_pairs={{0,2},{1,3},{2,0},{3,1},{4,6},{5,7},{6,4},{7,5},{8,10},{9,11},{10,... | collective-permute-start | bytes 1179656 | tf_op jit(solution)/shard_map/ppermute | solution.py:206
  5.4 6.0 %copy-start = (bf16[1,96,2048]{2,1,0:T(8,128)(2,1)S(1)}, bf16[1,96,2048]{2,1,0:T(8,128)(2,1)}, u32[]{:S(2)}) copy-start(bf16[1,96,2048]{2,1,0:T(8,128)(2,1)} %param.15) | copy-start | bytes 1179652
  5.4 17.5 %copy-start.2 = (f32[128,2]{0,1:T(2,128)S(1)}, f32[128,2]{0,1:T(2,128)}, u32[]{:S(2)}) copy-start(f32[128,2]{0,1:T(2,128)} %param.12) | copy-start | bytes 3076
  5.4 19.0 %all-to-all-start = ((bf16[8,24,1024]{2,1,0:T(8,128)(2,1)}), bf16[8,24,1024]{2,1,0:T(8,128)(2,1)S(1)}, u32[]{:S(2)}, u32[]{:S(2)}) async-start(bf16[8,24,1024]{2,1,0:T(8,128)(2,1)} %bitcast.6), calls=%async_computation | async-start | bytes 786432 | tf_op jit(solution)/shard_map/all_to_all | solution.py:218
  11.4 11.6 %collective-permute-start.4 = (bf16[96,2048]{1,0:T(8,128)(2,1)S(1)}, bf16[96,2048]{1,0:T(8,128)(2,1)S(1)}, u32[]{:S(2)}, u32[]{:S(2)}) collective-permute-start(bf16[96,2048]{1,0:T(8,128)(2,1)S(1)} %bitcast.18), channel_id=1, source_target_pairs={{0,2},{1,3},{2,0},{3,1},{4,6},{5,7},{6,4},{7,5},{8,10},{9,11},{10,... | collective-permute-start | bytes 1179656 | tf_op jit(solution)/shard_map/ppermute | solution.py:207
  12.0 12.4 %collective-permute-start.1 = (bf16[2,96,1024]{2,1,0:T(8,128)(2,1)S(1)}, bf16[2,96,1024]{2,1,0:T(8,128)(2,1)S(1)}, u32[]{:S(2)}, u32[]{:S(2)}) collective-permute-start(bf16[2,96,1024]{2,1,0:T(8,128)(2,1)S(1)} %get-tuple-element.15.keep_ref), channel_id=1, source_target_pairs={{0,1},{1,0},{2,3},{3,2},{4,5},{5,4},{6,7},{7,6},{8,9},{9,8},{10,11... | collective-permute-start | bytes 1179656 | tf_op jit(solution)/shard_map/ppermute | solution.py:208
  15.4 9.0 %collective-permute-start.2 = (bf16[2,96,1024]{2,1,0:T(8,128)(2,1)S(1)}, bf16[2,96,1024]{2,1,0:T(8,128)(2,1)}, u32[]{:S(2)}, u32[]{:S(2)}) collective-permute-start(bf16[2,96,1024]{2,1,0:T(8,128)(2,1)S(1)} %collective-permute-done.far_ref), channel_id=1, source_target_pairs={{0,1},{1,0},{2,3},{3,2},{4,5},{5,4},{6,7},{7,6},{8,9},{9,8},{10,11... | collective-permute-start | bytes 1179656 | tf_op jit(solution)/shard_map/ppermute | solution.py:210
  15.4 12.6 %collective-permute-start.5 = (bf16[96,2048]{1,0:T(8,128)(2,1)S(1)}, bf16[96,2048]{1,0:T(8,128)(2,1)S(1)}, u32[]{:S(2)}, u32[]{:S(2)}) collective-permute-start(bf16[96,2048]{1,0:T(8,128)(2,1)S(1)} %bitcast.19), channel_id=1, source_target_pairs={{0,1},{1,0},{2,3},{3,2},{4,5},{5,4},{6,7},{7,6},{8,9},{9,8},{10,11... | collective-permute-start | bytes 1179656 | tf_op jit(solution)/shard_map/ppermute | solution.py:209
  22.9 5.0 %collective-permute-start.6 = (bf16[96,2048]{1,0:T(8,128)(2,1)S(1)}, bf16[96,2048]{1,0:T(8,128)(2,1)S(1)}, u32[]{:S(2)}, u32[]{:S(2)}) collective-permute-start(bf16[96,2048]{1,0:T(8,128)(2,1)S(1)} %collective-permute-done.4.far_ref), channel_id=1, source_target_pairs={{0,1},{1,0},{2,3},{3,2},{4,5},{5,4},{6,7},{7,6},{8,9},{9,8},{10,11... | collective-permute-start | bytes 1179656 | tf_op jit(solution)/shard_map/ppermute | solution.py:211
  22.9 0.7 %copy-start.1 = (s32[128,2]{0,1:T(2,128)S(1)}, s32[128,2]{0,1:T(2,128)}, u32[]{:S(2)}) copy-start(s32[128,2]{0,1:T(2,128)} %param.10) | copy-start | bytes 3076
  23.0 0.7 %copy-start.3 = (f32[128]{0:T(128)S(1)}, f32[128]{0:T(128)}, u32[]{:S(2)}) copy-start(f32[128]{0:T(128)} %param.11) | copy-start | bytes 1540
  26.2 6.3 %collective-permute-start.3 = (bf16[96,768]{1,0:T(8,128)(2,1)S(1)}, bf16[96,768]{1,0:T(8,128)(2,1)S(1)}, u32[]{:S(2)}, u32[]{:S(2)}) collective-permute-start(bf16[96,768]{1,0:T(8,128)(2,1)S(1)} %get-tuple-element.18), channel_id=1, source_target_pairs={{0,2},{1,3},{2,0},{3,1},{4,6},{5,7},{6,4},{7,5},{8,10},{9,11},{10,... | collective-permute-start | bytes 442376 | tf_op jit(solution)/shard_map/ppermute | solution.py:227
